TPU v7x, 32 devices: a whole 2x2x4 slice. The times are simulated.
32 devices in a mesh: grp: 2 (over y), ep: 4 (over z), tp: 4 (over x, core).
Axes of the slice: x: 2, y: 2, z: 4, core: 2. Of those that a mesh axis runs over, the one named last changes fastest.
Arguments:
- hidden_in: bfloat16 [4096, 2048], P(('grp', 'ep', 'tp')), parts along dimension 0, may hold values from -6 to 6
- expert_ids: int32 [4096, 2], P(('grp', 'ep', 'tp')), parts along dimension 0, may hold values from 0 to 15, all different within a row; in each aligned block of 128 rows (0 to 127, 128 to 255, ...) at most 32 rows name the same one
- route_weights: float32 [4096, 2], P(('grp', 'ep', 'tp')), parts along dimension 0, may hold values from 0.1 to 1
- norm_gain: float32 [2048], replicated, may hold values from 0.1 to 1.9
- gate_proj: bfloat16 [16, 2048, 512], P(('ep', 'tp')), may hold values from -0.125 to 0.125
- up_proj: bfloat16 [16, 2048, 512], P(('ep', 'tp')), may hold values from -0.125 to 0.125
- down_proj: bfloat16 [16, 512, 2048], P(('ep', 'tp')), may hold values from -0.25 to 0.25
Outputs:
- mixed_out: bfloat16 [4096, 2048], P(('grp', 'ep', 'tp')), parts along dimension 0
There are 2 independent parts, one for each index of `grp`. A program takes and returns all parts, laid end to end along the dimension named above; an argument that names none is the same for every part. Nothing has to cross between parts.
Inputs may be any that keep to these rules, and one draw needn't show every extreme that they name: `expert_ids`: each token names 2 different experts; among the 128 tokens of one device (aligned blocks of rows) no expert is named more than 32 times, and in every draw some expert is named exactly 32 times by some device's tokens.
All inputs are finite; a program needn't handle non-finite values.
Results may differ from a plain program's by a relative error of at most 0.0071.
Values may be sent and summed in bfloat16 or wider, within the bound.
No kernel may reach another device: no remote copies, remote signals or barrier semaphores. Data moves between devices by JAX's collectives and lax.ppermute only.
A program may use at most 64 MiB of HBM per device.

v0:
```python
import jax
import jax.numpy as jnp
from jax import lax
from jax.sharding import PartitionSpec as P


def body(hidden_in, expert_ids, route_weights, norm_gain, gate_proj, up_proj, down_proj):
    token_count = hidden_in.shape[0]
    model_width = hidden_in.shape[1]
    choose_count = expert_ids.shape[1]
    ep_count = lax.axis_size("ep")
    tp_count = lax.axis_size("tp")
    expert_count = ep_count * tp_count
    capacity = max(2, 2 * choose_count * token_count // expert_count)
    as_float = hidden_in.astype(jnp.float32)
    scaled = as_float * lax.rsqrt(jnp.mean(as_float * as_float, axis=-1, keepdims=True) + 1e-06)
    normed = (scaled * norm_gain).astype(jnp.bfloat16)
    flat_ids = expert_ids.reshape(-1)
    onehot = (flat_ids[:, None] == jnp.arange(expert_count, dtype=jnp.int32)[None, :]).astype(
        jnp.int32
    )
    slot_index = jnp.sum((jnp.cumsum(onehot, axis=0) - onehot) * onehot, axis=1)
    target = flat_ids * capacity + slot_index
    routed = jnp.repeat(normed, choose_count, axis=0)
    buffer = jnp.zeros((expert_count * capacity, model_width), jnp.bfloat16).at[target].set(routed)
    buffer = buffer.reshape(expert_count, capacity, model_width)
    arrived = lax.all_to_all(buffer, ("ep", "tp"), split_axis=0, concat_axis=0, tiled=True)
    shape_in = arrived.shape
    block_in = arrived.reshape(-1, model_width)
    gate_act = jnp.dot(block_in, gate_proj[0], preferred_element_type=jnp.float32)
    up_act = jnp.dot(block_in, up_proj[0], preferred_element_type=jnp.float32)
    hidden = (jax.nn.silu(gate_act) * up_act).astype(jnp.bfloat16)
    result = jnp.dot(hidden, down_proj[0], preferred_element_type=jnp.float32).astype(jnp.bfloat16)
    results = result.reshape(shape_in)
    returned = lax.all_to_all(results, ("ep", "tp"), split_axis=0, concat_axis=0, tiled=True)
    picked = returned.reshape(-1, model_width)[target].astype(jnp.float32)
    picked = picked.reshape(token_count, choose_count, model_width)
    return jnp.sum(picked * route_weights[:, :, None], axis=1).astype(jnp.bfloat16)


def solution(mesh):
    return jax.shard_map(
        body,
        mesh=mesh,
        in_specs=(
            P(("grp", "ep", "tp"), None),
            P(("grp", "ep", "tp"), None),
            P(("grp", "ep", "tp"), None),
            P(),
            P(("ep", "tp"), None, None),
            P(("ep", "tp"), None, None),
            P(("ep", "tp"), None, None),
        ),
        out_specs=P(("grp", "ep", "tp"), None),
        check_vma=False,
    )
```

profile of v0, /device:TPU:11, one launch (start us, length us, event | category | flops | bytes accessed | tf_op | source)
XLA Modules:
  0.0 139.3 jit_solution(16366005023959419473)
XLA Ops:
  0.0 0.9 copy.10
  0.9 0.1 eq.29
  1.1 0.1 eq.25
  1.2 0.7 broadcast_multiply_fusion
  1.9 0.6 reduce-window.6
  2.5 0.2 slice_reduce_fusion
  2.7 0.1 copy.9
  2.8 0.1 mul.55
  3.0 1.2 fusion.11
  4.2 1.2 fusion.13
  5.5 0.6 broadcast_in_dim.5
  6.1 1.2 reshape.94
  7.3 0.1 fusion.21
  7.4 4.4 %scatter_custom_fusion = bf16[512,2048]{1,0:T(8,128)(2,1)} fusion(s32[256]{0:T(256)S(1)} %bitcast.46, bf16[256,2048]{1,0:T(8,128)(2,1)} %reshape.94, bf16[]{:T(256)} %constant.8.clone.1), kind=kCustom, calls=%fused_computation.16 | custom fusion | bytes 2097664 | tf_op jit(solution)/shard_map/scatter | solution.py:25
  11.9 53.9 %all_to_all.10 = bf16[16,32,2048]{2,1,0:T(8,128)(2,1)S(1)} all-to-all(bf16[16,32,2048]{2,1,0:T(8,128)(2,1)} %bitcast.42), channel_id=1, replica_groups=mesh['grp'=2,'ep'=4,'tp'=4] {'ep','tp'}, dimensions={0} | all-to-all | bytes 4194304 | tf_op jit(solution)/shard_map/all_to_all | solution.py:27
  65.8 1.3 copy-done.1
  67.1 1.2 fusion.3
  68.3 6.1 %convolution_convert_fusion = bf16[512,2048]{1,0:T(8,128)(2,1)} fusion(bf16[1,512,2048]{2,1,0:T(8,128)(2,1)S(1)} %copy-done, bf16[512,2048]{1,0:T(8,128)(2,1)} %bitcast.45, bf16[1,2048,512]{2,1,0:T(8,128)(2,1)} %param.12, f32[512,512]{1,0:T(8,128)S(1)} %fusion.3), kind=kOutput, calls=%fused_computation.2 | convolution fusion | flops 2150105088 | bytes 9437184 | tf_op jit(solution)/shard_map/dot_general | solution.py:33
  74.4 5.2 %all-to-all-start.1 = ((bf16[16,32,2048]{2,1,0:T(8,128)(2,1)}), bf16[16,32,2048]{2,1,0:T(8,128)(2,1)}, u32[]{:S(2)}, u32[]{:S(2)}) async-start(bf16[16,32,2048]{2,1,0:T(8,128)(2,1)} %bitcast.43), calls=%async_computation.1 | async-start | bytes 4194304 | tf_op jit(solution)/shard_map/all_to_all | solution.py:35
  79.6 0.1 copy.13
  79.7 47.4 %all-to-all-done.1 = bf16[16,32,2048]{2,1,0:T(8,128)(2,1)} async-done(((bf16[16,32,2048]{2,1,0:T(8,128)(2,1)}), bf16[16,32,2048]{2,1,0:T(8,128)(2,1)}, u32[]{:S(2)}, u32[]{:S(2)}) %all-to-all-start.1) | async-done | bytes 2097184 | tf_op jit(solution)/shard_map/all_to_all | solution.py:35
  127.1 4.2 %gather_fusion = bf16[256,2048]{1,0:T(8,128)(2,1)S(1)} fusion(bf16[512,2048]{1,0:T(8,128)(2,1)} %bitcast.9, s32[1024]{0:T(1024)S(1)} %pad_clamp_fusion), kind=kCustom, calls=%fused_computation | custom fusion | bytes 2098176 | tf_op jit(solution)/shard_map/gather | solution.py:36
  131.3 2.4 %reshape.81 = f32[128,2,2048]{2,1,0:T(2,128)} reshape(bf16[256,2048]{1,0:T(8,128)(2,1)S(1)} %gather_fusion) | data formatting | bytes 3145728 | tf_op jit(solution)/shard_map/convert_element_type | solution.py:36
  133.7 5.6 %multiply_reduce_fusion = bf16[128,2048]{1,0:T(8,128)(2,1)} fusion(f32[128,2,2048]{2,1,0:T(2,128)} %reshape.81, f32[128,2]{1,0:T(8,128)S(1)} %copy.13), kind=kLoop, calls=%fused_computation.8 | loop fusion | flops 786432 | bytes 2622464 | tf_op jit(solution)/shard_map/reduce_sum | solution.py:38
  (13 shorter events, 0.1 us)
Async XLA Ops:
  0.0 68.3 %copy-start = (bf16[1,512,2048]{2,1,0:T(8,128)(2,1)S(1)}, bf16[1,512,2048]{2,1,0:T(8,128)(2,1)}, u32[]{:S(2)}) copy-start(bf16[1,512,2048]{2,1,0:T(8,128)(2,1)} %param.13) | copy-start | bytes 6291460
  11.9 55.2 %copy-start.3 = (bf16[1,2048,512]{2,1,0:T(8,128)(2,1)S(1)}, bf16[1,2048,512]{2,1,0:T(8,128)(2,1)}, u32[]{:S(2)}) copy-start(bf16[1,2048,512]{2,1,0:T(8,128)(2,1)} %param.11) | copy-start | bytes 6291460
  65.8 1.3 copy-start.1
  74.4 5.2 %copy-start.2 = (f32[128,2]{0,1:T(2,128)S(1)}, f32[128,2]{0,1:T(2,128)}, u32[]{:S(2)}) copy-start(f32[128,2]{0,1:T(2,128)} %param.9) | copy-start | bytes 3076
  74.4 52.7 %all-to-all-start.1 = ((bf16[16,32,2048]{2,1,0:T(8,128)(2,1)}), bf16[16,32,2048]{2,1,0:T(8,128)(2,1)}, u32[]{:S(2)}, u32[]{:S(2)}) async-start(bf16[16,32,2048]{2,1,0:T(8,128)(2,1)} %bitcast.43), calls=%async_computation.1 | async-start | bytes 4194304 | tf_op jit(solution)/shard_map/all_to_all | solution.py:35
where the time goes:
time: 140 us; the launch traced here: 139 us
  blocking collectives  53.9 us (38%)
  waiting for transfers between devices  47.4 us (34%)
  local copies, waits for them, and re-layouts  16 us (11%)
  other arithmetic  9.47 us (7%)
  matrix products  7.31 us (5%)
  starting transfers between devices  5.16 us (4%)
    all_to_all x1, blocking collectives, body(): lax.all_to_all(buffer, ('ep', 'tp'), split_axis=0, concat_axis=0, tiled=T...  53.9 us
    all_to_all x1, waiting for transfers between devices, body(): lax.all_to_all(results, ('ep', 'tp'), split_axis=0, concat_axis=0, tiled=...  47.4 us
    dot_general x1, matrix products, body(): jnp.dot(hidden, down_proj[0], preferred_element_type=jnp.float32)  6.06 us
    reduce_sum x1, other arithmetic, body(): jnp.sum(picked * route_weights[:, :, None], axis=1).astype(jnp.bfloat16)  5.59 us
    all_to_all x1, starting transfers between devices, body(): lax.all_to_all(results, ('ep', 'tp'), split_axis=0, concat_axis=0, tiled=...  5.16 us
    scatter x1, local copies, waits for them, and re-layouts, body(): jnp.zeros((expert_count * capacity, model_width), jnp.bfloat16).at[target]  4.43 us
    gather x1, local copies, waits for them, and re-layouts, body(): picked = returned.reshape(-1, model_width)[target].astype(jnp.float32)  4.22 us
  transfers between devices with their start and end apart: 1, of which 1 were waited for; matrix products, arithmetic and copies ran while one was open for 0% of the time, Pallas kernels for 0%

commit v1 on v0

v1 whole, which is shorter than its diff:
```python
import functools

import jax
import jax.numpy as jnp
from jax import lax
from jax.experimental import pallas as pl
from jax.experimental.pallas import tpu as pltpu
from jax.sharding import PartitionSpec as P


def targets_of(ids_ref, expert_count, capacity):
    choose_count, token_count = ids_ref.shape
    experts = lax.broadcasted_iota(jnp.int32, (expert_count, token_count), 0)
    named = [ids_ref[k : k + 1, :] == experts for k in range(choose_count)]
    either = functools.reduce(jnp.logical_or, named).astype(jnp.float32).astype(jnp.bfloat16)
    earlier = lax.broadcasted_iota(jnp.int32, (token_count, token_count), 0) < (
        lax.broadcasted_iota(jnp.int32, (token_count, token_count), 1)
    )
    earlier = earlier.astype(jnp.float32).astype(jnp.bfloat16)
    before = jnp.dot(either, earlier, preferred_element_type=jnp.float32)
    targets = []
    for k in range(choose_count):
        slot = jnp.sum(jnp.where(named[k], before, 0.0), axis=0, keepdims=True)
        targets.append(ids_ref[k : k + 1, :] * capacity + slot.astype(jnp.int32))
    return targets


def as_ones(mask):
    return mask.astype(jnp.float32).astype(jnp.bfloat16)


def dispatch_kernel(expert_count, capacity, hidden_ref, ids_ref, gain_ref, buffer_ref):
    as_float = hidden_ref[...].astype(jnp.float32)
    mean = jnp.mean(as_float * as_float, axis=-1, keepdims=True)
    normed = (as_float * lax.rsqrt(mean + 1e-06) * gain_ref[...]).astype(jnp.bfloat16)
    targets = targets_of(ids_ref, expert_count, capacity)
    rows = lax.broadcasted_iota(jnp.int32, (expert_count * capacity, ids_ref.shape[1]), 0)
    chosen = as_ones(functools.reduce(jnp.logical_or, [rows == target for target in targets]))
    buffer_ref[...] = jnp.dot(chosen, normed, preferred_element_type=jnp.float32).astype(jnp.bfloat16)


def expert_kernel(rows_ref, gate_ref, up_ref, down_ref, out_ref):
    block = rows_ref[...]
    gate_act = jnp.dot(block, gate_ref[0], preferred_element_type=jnp.float32)
    up_act = jnp.dot(block, up_ref[0], preferred_element_type=jnp.float32)
    hidden = (gate_act / (1.0 + jnp.exp(-gate_act)) * up_act).astype(jnp.bfloat16)
    out_ref[...] = jnp.dot(hidden, down_ref[0], preferred_element_type=jnp.float32).astype(jnp.bfloat16)


def combine_kernel(expert_count, capacity, rows_ref, ids_ref, weights_ref, out_ref):
    token_count = ids_ref.shape[1]
    targets = targets_of(ids_ref, expert_count, capacity)
    rows = lax.broadcasted_iota(jnp.int32, (expert_count * capacity, token_count), 0)
    total = None
    for k, target in enumerate(targets):
        picked = lax.dot_general(
            as_ones(rows == target), rows_ref[...], (((0,), (0,)), ((), ())), preferred_element_type=jnp.float32
        )
        weight = jnp.broadcast_to(weights_ref[k : k + 1, :], (8, token_count)).T[:, 0:1]
        total = picked * weight if total is None else total + picked * weight
    out_ref[...] = total.astype(jnp.bfloat16)


def whole(*arrays):
    return [pl.BlockSpec(a.shape, lambda *_, n=len(a.shape): (0,) * n) for a in arrays]


def body(hidden_in, expert_ids, route_weights, norm_gain, gate_proj, up_proj, down_proj):
    token_count, model_width = hidden_in.shape
    choose_count = expert_ids.shape[1]
    expert_count = lax.axis_size("ep") * lax.axis_size("tp")
    capacity = max(2, 2 * choose_count * token_count // expert_count)
    slots = expert_count * capacity
    ids, weights, gain = expert_ids.T, route_weights.T, norm_gain[None, :]
    buffer = pl.pallas_call(
        functools.partial(dispatch_kernel, expert_count, capacity),
        out_shape=jax.ShapeDtypeStruct((slots, model_width), jnp.bfloat16),
        name="dispatch",
    )(hidden_in, ids, gain)
    buffer = buffer.reshape(expert_count, capacity, model_width)
    arrived = lax.all_to_all(buffer, ("ep", "tp"), split_axis=0, concat_axis=0, tiled=True)
    arrived = arrived.reshape(slots, model_width)
    tile = slots // 2 if slots % 32 == 0 else slots
    result = pl.pallas_call(
        expert_kernel,
        grid=(slots // tile,),
        in_specs=[pl.BlockSpec((tile, model_width), lambda i: (i, 0)), *whole(gate_proj, up_proj, down_proj)],
        out_specs=pl.BlockSpec((tile, model_width), lambda i: (i, 0)),
        out_shape=jax.ShapeDtypeStruct((slots, model_width), jnp.bfloat16),
        name="experts",
    )(arrived, gate_proj, up_proj, down_proj)
    results = result.reshape(expert_count, capacity, model_width)
    returned = lax.all_to_all(results, ("ep", "tp"), split_axis=0, concat_axis=0, tiled=True)
    return pl.pallas_call(
        functools.partial(combine_kernel, expert_count, capacity),
        out_shape=jax.ShapeDtypeStruct((token_count, model_width), jnp.bfloat16),
        name="combine",
    )(returned.reshape(slots, model_width), ids, weights)


def solution(mesh):
    return jax.shard_map(
        body,
        mesh=mesh,
        in_specs=(
            P(("grp", "ep", "tp"), None),
            P(("grp", "ep", "tp"), None),
            P(("grp", "ep", "tp"), None),
            P(),
            P(("ep", "tp"), None, None),
            P(("ep", "tp"), None, None),
            P(("ep", "tp"), None, None),
        ),
        out_specs=P(("grp", "ep", "tp"), None),
        check_vma=False,
    )
```

time: 140 us -> 122 us (0.87)
  blocking collectives: 53.9 us -> 106 us
  waiting for transfers between devices: 47.4 us -> 0 us
  local copies, waits for them, and re-layouts: 16 us -> 0 us
  Pallas kernels: 0 us -> 14.5 us
  other arithmetic: 9.47 us -> 0 us
  matrix products: 7.31 us -> 0 us
  starting transfers between devices: 5.16 us -> 0 us
    all_to_all x0 -> x1, blocking collectives: none -> 52.4 us  [body(): lax.all_to_all(results, ('ep', 'tp'), split_axis=0, concat_axis=0, tiled=...]
    all_to_all x1 -> x0, waiting for transfers between devices: 47.4 us -> none  [body(): lax.all_to_all(results, ('ep', 'tp'), split_axis=0, concat_axis=0, tiled=...]
    pallas_call x0 -> x3, Pallas kernels: none -> 14.5 us  [the longest x1 7.94 us: body(): pl.pallas_call(expert_kernel, grid=(slots // tile,), in_specs=[pl.BlockSp...]
    dot_general x2 -> x0, matrix products: 7.31 us -> none  [the longest x1 6.06 us: body(): jnp.dot(hidden, down_proj[0], preferred_element_type=jnp.float32)]
    reduce_sum x3 -> x0, other arithmetic: 6.91 us -> none  [the longest x1 5.59 us: body(): jnp.sum(picked * route_weights[:, :, None], axis=1).astype(jnp.bfloat16)]
    all_to_all x1 -> x0, starting transfers between devices: 5.16 us -> none  [body(): lax.all_to_all(results, ('ep', 'tp'), split_axis=0, concat_axis=0, tiled=...]
    scatter x1 -> x0, local copies, waits for them, and re-layouts: 4.43 us -> none  [body(): jnp.zeros((expert_count * capacity, model_width), jnp.bfloat16).at[target]]
    gather x1 -> x0, local copies, waits for them, and re-layouts: 4.22 us -> none  [body(): picked = returned.reshape(-1, model_width)[target].astype(jnp.float32)]
  transfers between devices with their start and end apart: 1 -> 0, of which waited for: 1 -> 0; matrix products, arithmetic and copies ran while one was open for 0% -> 0% of each run, Pallas kernels for 0% -> 0%
where the time goes in v1:
time: 122 us; the launch traced here: 121 us
  blocking collectives  106 us (87%)
  Pallas kernels  14.5 us (12%)
    all_to_all x1, blocking collectives, body(): lax.all_to_all(buffer, ('ep', 'tp'), split_axis=0, concat_axis=0, tiled=T...  53.9 us
    all_to_all x1, blocking collectives, body(): lax.all_to_all(results, ('ep', 'tp'), split_axis=0, concat_axis=0, tiled=...  52.4 us
    pallas_call x1, Pallas kernels, body(): pl.pallas_call(expert_kernel, grid=(slots // tile,), in_specs=[pl.BlockSp...  7.94 us
    pallas_call x1, Pallas kernels, body(): pl.pallas_call(functools.partial(combine_kernel, expert_count, capacity),...  3.35 us
    pallas_call x1, Pallas kernels, body(): pl.pallas_call(functools.partial(dispatch_kernel, expert_count, capacity)...  3.25 us

profile of v1, /device:TPU:11, one launch (start us, length us, event | category | flops | bytes accessed | tf_op | source)
XLA Modules:
  0.0 120.8 jit_solution(18122323601818953610)
XLA Ops:
  0.0 3.2 %dispatch.1 = bf16[512,2048]{1,0:T(8,128)(2,1)} custom-call(bf16[128,2048]{1,0:T(8,128)(2,1)} %hidden_ref.1, s32[2,128]{1,0:T(2,128)} %bitcast.12, f32[1,2048]{1,0:T(1,128)} %bitcast.11), custom_call_target="tpu_custom_call" | custom-call | tf_op jit(solution)/shard_map/dispatch/pallas_call | solution.py:75
  3.2 53.9 %all_to_all.10 = bf16[16,32,2048]{2,1,0:T(8,128)(2,1)} all-to-all(bf16[16,32,2048]{2,1,0:T(8,128)(2,1)} %bitcast.10), channel_id=1, replica_groups=mesh['grp'=2,'ep'=4,'tp'=4] {'ep','tp'}, dimensions={0} | all-to-all | bytes 4194304 | tf_op jit(solution)/shard_map/all_to_all | solution.py:81
  57.1 7.9 %experts.1 = bf16[512,2048]{1,0:T(8,128)(2,1)} custom-call(bf16[512,2048]{1,0:T(8,128)(2,1)} %bitcast.7, bf16[1,2048,512]{2,1,0:T(8,128)(2,1)} %gate_ref.1, bf16[1,2048,512]{2,1,0:T(8,128)(2,1)} %up_ref.1, bf16[1,512,2048]{2,1,0:T(8,128)(2,1)} %down_ref.1), custom_call_target="tpu_custom_call" | custom-call | tf_op jit(solution)/shard_map/experts/pallas_call | solution.py:84
  65.1 52.4 %all_to_all.11 = bf16[16,32,2048]{2,1,0:T(8,128)(2,1)} all-to-all(bf16[16,32,2048]{2,1,0:T(8,128)(2,1)} %bitcast.8), channel_id=1, replica_groups=mesh['grp'=2,'ep'=4,'tp'=4] {'ep','tp'}, dimensions={0} | all-to-all | bytes 4194304 | tf_op jit(solution)/shard_map/all_to_all | solution.py:93
  117.5 3.3 %combine.1 = bf16[128,2048]{1,0:T(8,128)(2,1)} custom-call(bf16[512,2048]{1,0:T(8,128)(2,1)} %bitcast.9, s32[2,128]{1,0:T(2,128)} %bitcast.13, f32[2,128]{1,0:T(2,128)} %bitcast.14), custom_call_target="tpu_custom_call" | custom-call | tf_op jit(solution)/shard_map/combine/pallas_call | solution.py:94

commit v2 on v0

v2 whole, which is shorter than its diff:
```python
import functools

import jax
import jax.numpy as jnp
from jax import lax
from jax.experimental import pallas as pl
from jax.experimental.pallas import tpu as pltpu
from jax.sharding import Mesh, PartitionSpec as P


SMEM = pl.BlockSpec(memory_space=pltpu.SMEM)
VMEM = pl.BlockSpec(memory_space=pltpu.VMEM)
HBM = pl.BlockSpec(memory_space=pl.ANY)
LIMIT = pltpu.CompilerParams(vmem_limit_bytes=32 * 1024 * 1024)


def as_ones(mask):
    return mask.astype(jnp.float32).astype(jnp.bfloat16)


def any_of(masks):
    return functools.reduce(jnp.logical_or, masks)


def slots_of(ids, expert_count):
    choose_count, token_count = ids.shape
    experts = lax.broadcasted_iota(jnp.int32, (expert_count, token_count), 0)
    named = [ids[k : k + 1, :] == experts for k in range(choose_count)]
    earlier = as_ones(
        lax.broadcasted_iota(jnp.int32, (token_count, token_count), 0)
        < lax.broadcasted_iota(jnp.int32, (token_count, token_count), 1)
    )
    before = jnp.dot(as_ones(any_of(named)), earlier, preferred_element_type=jnp.float32)
    return [jnp.sum(jnp.where(mask, before, 0.0), axis=0, keepdims=True).astype(jnp.int32) for mask in named]


def marks_of(ids, slots, first, turn, count, capacity):
    rows = lax.broadcasted_iota(jnp.int32, (count * capacity, ids.shape[1]), 0)
    targets = []
    for k, slot in enumerate(slots):
        expert = ids[k : k + 1, :] - first
        inside = (expert >= 0) & (expert < count)
        targets.append(jnp.where(inside, (expert ^ turn) * capacity + slot, -1))
    return [rows == target for target in targets]


def column_of(row):
    return jnp.broadcast_to(row, (8, row.shape[1])).T[:, 0:1]


def pick(marks, weights, rows):
    total = None
    for k, mark in enumerate(marks):
        picked = lax.dot_general(mark, rows, (((0,), (0,)), ((), ())), preferred_element_type=jnp.float32)
        picked = picked * column_of(weights[k : k + 1, :])
        total = picked if total is None else total + picked
    return total


def together(refs):
    return jnp.concatenate([ref[...] for ref in refs], axis=0) if len(refs) > 1 else refs[0][...]


def apart(value, refs):
    size = value.shape[0] // len(refs)
    for i, ref in enumerate(refs):
        ref[...] = value[i * size : (i + 1) * size].astype(ref.dtype)


def norm_kernel(hidden_ref, gain_ref, ids_ref, weights_ref, out_ref):
    as_float = hidden_ref[...].astype(jnp.float32)
    scale = lax.rsqrt(jnp.mean(as_float * as_float, axis=-1, keepdims=True) + 1e-06)
    width = hidden_ref.shape[1]
    out_ref[:, :width] = (as_float * scale * gain_ref[...]).astype(jnp.bfloat16)
    facts, left = [ids_ref[...].astype(jnp.float32)], weights_ref[...]
    for _ in range(3):
        term = left.astype(jnp.bfloat16).astype(jnp.float32)
        facts.append(term)
        left = left - term
    facts.append(jnp.zeros((LANES - 4 * ids_ref.shape[0], ids_ref.shape[1]), jnp.float32))
    out_ref[:, width:] = jnp.concatenate(facts, axis=0).T.astype(jnp.bfloat16)


def facts_of(block_ref, choose_count):
    facts = block_ref[:, block_ref.shape[1] - LANES :].astype(jnp.float32).T
    terms = [facts[(1 + i) * choose_count : (2 + i) * choose_count, :] for i in range(3)]
    return facts[:choose_count, :].astype(jnp.int32), terms[0] + terms[1] + terms[2]


def pack_kernel(layout, keep, place_ref, block_ref, *refs):
    choose_count, expert_count, count, capacity = layout
    ids, weights = facts_of(block_ref, choose_count)
    marks = marks_of(ids, slots_of(ids, expert_count), place_ref[0], place_ref[1], count, capacity)
    if keep:
        for k, mark in enumerate(marks):
            refs[0][k] = as_ones(mark)
        refs[1][...] = weights
    rows = block_ref[:, : block_ref.shape[1] - LANES]
    apart(jnp.dot(as_ones(any_of(marks)), rows, preferred_element_type=jnp.float32), refs[2 * keep :])


def mark_kernel(layout, place_ref, ids_ref, out_ref):
    _, expert_count, count, capacity = layout
    ids = ids_ref[...]
    marks = marks_of(ids, slots_of(ids, expert_count), place_ref[0], place_ref[1], count, capacity)
    for k, mark in enumerate(marks):
        out_ref[k] = as_ones(mark)


def expert_kernel(count, *refs):
    weight_refs, in_refs, out_refs = refs[:3], refs[3 : 3 + count], refs[3 + count : 3 + 2 * count]
    *held, sems = refs[3 + 2 * count :]
    loads = [pltpu.make_async_copy(weight_refs[i].at[0], held[i], sems.at[i]) for i in range(3)]
    for load in loads:
        load.start()
    rows = together(in_refs)
    loads[0].wait()
    gate_act = jnp.dot(rows, held[0][...], preferred_element_type=jnp.float32)
    loads[1].wait()
    up_act = jnp.dot(rows, held[1][...], preferred_element_type=jnp.float32)
    hidden = (gate_act / (1.0 + jnp.exp(-gate_act)) * up_act).astype(jnp.bfloat16)
    loads[2].wait()
    apart(jnp.dot(hidden, held[2][...], preferred_element_type=jnp.float32), out_refs)


def partial_kernel(weights_ref, marks_ref, *refs):
    out = pick([marks_ref[k] for k in range(marks_ref.shape[0])], weights_ref[...], together(refs[:-1]))
    refs[-1][...] = out.astype(jnp.bfloat16)


def final_kernel(weights_ref, marks_ref, partial_ref, *refs):
    near = pick([marks_ref[k] for k in range(marks_ref.shape[0])], weights_ref[...], together(refs[:-1]))
    refs[-1][...] = (near + partial_ref[...].astype(jnp.float32)).astype(jnp.bfloat16)


LANES = 128


def body(hidden_in, expert_ids, route_weights, norm_gain, gate_proj, up_proj, down_proj):
    token_count, model_width = hidden_in.shape
    choose_count = expert_ids.shape[1]
    half_count = lax.axis_size("el") * lax.axis_size("tp")
    expert_count = lax.axis_size("eh") * half_count
    capacity = max(2, 2 * choose_count * token_count // expert_count)
    slots = half_count * capacity
    group = ("el", "tp")
    paired = half_count <= 8 and half_count & (half_count - 1) == 0 and capacity % 16 == 0
    turn = lax.axis_index(group) if paired else jnp.int32(0)
    place = jnp.stack([lax.axis_index("eh") * half_count, turn]).astype(jnp.int32)
    ids, weights, gain = expert_ids.T, route_weights.T, norm_gain[None, :]
    proj = [pltpu.with_memory_space_constraint(w, pltpu.HBM) for w in (gate_proj, up_proj, down_proj)]

    def array(*shape):
        return pltpu.HBM(shape, jnp.bfloat16)

    def call(kernel, scalars, out, *args, limit=LIMIT):
        return pl.pallas_call(
            kernel,
            in_specs=[SMEM] * scalars + [VMEM] * (len(args) - scalars),
            out_specs=[VMEM] * len(out),
            out_shape=out,
            compiler_params=limit,
        )(*args)

    def cross(value):
        return lax.ppermute(value, "eh", [(0, 1), (1, 0)])

    def scatter(parts):
        if not paired:
            blocks = parts[0].reshape(half_count, capacity, model_width)
            blocks = lax.all_to_all(blocks, group, split_axis=0, concat_axis=0, tiled=True)
            return [blocks.reshape(slots, model_width)]
        moved = [parts[0]]
        for j in range(1, len(parts)):
            moved.append(lax.ppermute(parts[j], group, [(i, i ^ j) for i in range(half_count)]))
        return moved

    def experts(rows):
        return pl.pallas_call(
            functools.partial(expert_kernel, len(rows)),
            in_specs=[HBM] * 3 + [VMEM] * len(rows),
            out_specs=[VMEM] * len(rows),
            out_shape=[array(*r.shape) for r in rows],
            scratch_shapes=[
                *[pltpu.VMEM(w.shape[1:], w.dtype) for w in proj],
                pltpu.SemaphoreType.DMA((3,)),
            ],
            compiler_params=LIMIT,
        )(*proj, *rows)

    pieces = half_count if paired else 1
    piece = array(slots // pieces, model_width)
    marks = array(choose_count, slots, token_count)
    layout = (choose_count, expert_count, half_count, capacity)
    (block,) = call(
        norm_kernel, 0, [array(token_count, model_width + LANES)], hidden_in, gain, ids, weights, limit=None
    )
    far_block = cross(block)
    kernel = functools.partial(pack_kernel, layout, False)
    near = scatter(call(kernel, 1, [piece] * pieces, place, block, limit=None))
    (near_marks,) = call(functools.partial(mark_kernel, layout), 1, [marks], place, ids)
    far_marks, far_weights, *far = call(
        functools.partial(pack_kernel, layout, True),
        1,
        [marks, pltpu.HBM((choose_count, token_count), jnp.float32)] + [piece] * pieces,
        place, far_block,
    )
    far = scatter(far)
    near = experts(near)
    far = experts(far)
    far = scatter(far)
    near = scatter(near)
    (partial,) = call(partial_kernel, 0, [array(token_count, model_width)], far_weights, far_marks, *far)
    partial = cross(partial)
    out = jax.ShapeDtypeStruct((token_count, model_width), jnp.bfloat16)
    return call(final_kernel, 0, [out], weights, near_marks, partial, *near)[0]


def solution(mesh):
    sizes = dict(mesh.shape)
    split = Mesh(mesh.devices.reshape(sizes["grp"], 2, sizes["ep"] // 2, sizes["tp"]), ("grp", "eh", "el", "tp"))
    rows, experts = P(("grp", "eh", "el", "tp"), None), P(("eh", "el", "tp"), None, None)

    def step(*args):
        return body(*args)

    step = jax.shard_map(
        step,
        mesh=split,
        in_specs=(rows, rows, rows, P(), experts, experts, experts),
        out_specs=rows,
        check_vma=False,
    )
    return step
```

time: 140 us -> 126 us (0.900)
  blocking collectives: 53.9 us -> 0 us
  starting transfers between devices: 5.16 us -> 33.9 us
  Pallas kernels: 0 us -> 20.3 us
  waiting for transfers between devices: 47.4 us -> 65.6 us
  local copies, waits for them, and re-layouts: 16 us -> 4.54 us
  other arithmetic: 9.47 us -> 0.07 us
  matrix products: 7.31 us -> 0 us
    ppermute x0 -> x30, waiting for transfers between devices: none -> 65.6 us  [the longest x28 41.2 us: scatter(): lax.ppermute(parts[j], group, [(i, i ^ j) for i in range(half_count)])]
    all_to_all x1 -> x0, blocking collectives: 53.9 us -> none  [body(): lax.all_to_all(buffer, ('ep', 'tp'), split_axis=0, concat_axis=0, tiled=T...]
    all_to_all x1 -> x0, waiting for transfers between devices: 47.4 us -> none  [body(): lax.all_to_all(results, ('ep', 'tp'), split_axis=0, concat_axis=0, tiled=...]
    ppermute x0 -> x30, starting transfers between devices: none -> 33.9 us  [the longest x28 28.6 us: scatter(): lax.ppermute(parts[j], group, [(i, i ^ j) for i in range(half_count)])]
    pallas_call x0 -> x8, Pallas kernels: none -> 20.3 us  [the longest x6 10.8 us: call(): pl.pallas_call(kernel, in_specs=[SMEM] * scalars + [VMEM] * (len(args) -...]
    dot_general x2 -> x0, matrix products: 7.31 us -> none  [the longest x1 6.06 us: body(): jnp.dot(hidden, down_proj[0], preferred_element_type=jnp.float32)]
    reduce_sum x3 -> x0, other arithmetic: 6.91 us -> none  [the longest x1 5.59 us: body(): jnp.sum(picked * route_weights[:, :, None], axis=1).astype(jnp.bfloat16)]
    all_to_all x1 -> x0, starting transfers between devices: 5.16 us -> none  [body(): lax.all_to_all(results, ('ep', 'tp'), split_axis=0, concat_axis=0, tiled=...]
  transfers between devices with their start and end apart: 1 -> 30, of which waited for: 1 -> 16; matrix products, arithmetic and copies ran while one was open for 0% -> 0% of each run, Pallas kernels for 0% -> 8%
where the time goes in v2:
time: 126 us; the launch traced here: 124 us
  waiting for transfers between devices  65.6 us (52%)
  starting transfers between devices  33.9 us (27%)
  Pallas kernels  20.3 us (16%)
  local copies, waits for them, and re-layouts  4.54 us (4%)
    ppermute x28, waiting for transfers between devices, scatter(): lax.ppermute(parts[j], group, [(i, i ^ j) for i in range(half_count)])  41.2 us
    ppermute x28, starting transfers between devices, scatter(): lax.ppermute(parts[j], group, [(i, i ^ j) for i in range(half_count)])  28.6 us
    ppermute x2, waiting for transfers between devices, cross(): return lax.ppermute(value, 'eh', [(0, 1), (1, 0)])  24.4 us
    pallas_call x6, Pallas kernels, call(): pl.pallas_call(kernel, in_specs=[SMEM] * scalars + [VMEM] * (len(args) -...  10.8 us
    pallas_call x2, Pallas kernels, experts(): pl.pallas_call(functools.partial(expert_kernel, len(rows)), in_specs=[HBM...  9.44 us
    ppermute x2, starting transfers between devices, cross(): return lax.ppermute(value, 'eh', [(0, 1), (1, 0)])  5.31 us
    unnamed x22, local copies, waits for them, and re-layouts  4.54 us
  transfers between devices with their start and end apart: 30, of which 16 were waited for; matrix products, arithmetic and copies ran while one was open for 0% of the time, Pallas kernels for 8%

profile of v2, /device:TPU:11, one launch (start us, length us, event | category | flops | bytes accessed | tf_op | source)
XLA Modules:
  0.0 124.4 jit_solution(11513011053060186155)
XLA Ops:
  0.0 2.1 %shard_map.74.block_ref = bf16[128,2176]{1,0:T(8,128)(2,1)} custom-call(bf16[128,2048]{1,0:T(8,128)(2,1)} %hidden_ref.1, f32[1,2048]{1,0:T(1,128)} %bitcast.9, s32[2,128]{1,0:T(2,128)} %bitcast.5, f32[2,128]{1,0:T(2,128)} %bitcast.7), custom_call_target="tpu_custom_call" | custom-call | tf_op jit(solution)/shard_map/pallas_call | solution.py:157
  2.1 2.3 %collective-permute-start = (bf16[128,2176]{1,0:T(8,128)(2,1)}, bf16[128,2176]{1,0:T(8,128)(2,1)S(1)}, u32[]{:S(2)}, u32[]{:S(2)}) collective-permute-start(bf16[128,2176]{1,0:T(8,128)(2,1)} %shard_map.74.block_ref), channel_id=1, source_target_pairs={{0,8},{8,0},{1,9},{9,1},{2,10},{10,2},{3,11},{11,3},{4,12},{12,4},... | collective-permute-start | bytes 1671176 | tf_op jit(solution)/shard_map/ppermute | solution.py:166
  4.5 24.4 %collective-permute-done.block_ref = bf16[128,2176]{1,0:T(8,128)(2,1)S(1)} collective-permute-done((bf16[128,2176]{1,0:T(8,128)(2,1)}, bf16[128,2176]{1,0:T(8,128)(2,1)S(1)}, u32[]{:S(2)}, u32[]{:S(2)}) %collective-permute-start) | collective-permute-done | bytes 557088 | tf_op jit(solution)/shard_map/ppermute | solution.py:166
  28.9 2.1 %shard_map.75 = (bf16[2,256,128]{2,1,0:T(8,128)(2,1)}, f32[2,128]{1,0:T(2,128)}, bf16[32,2048]{1,0:T(8,128)(2,1)}, bf16[32,2048]{1,0:T(8,128)(2,1)}, bf16[32,204...) custom-call(s32[2]{0:T(128)S(1)} %pad_add_fusion.place_ref, ...), custom_call_target="tpu_custom_call" | custom-call | tf_op jit(solution)/shard_map/pallas_call | solution.py:157
  36.7 2.1 %collective-permute-start.7 = (bf16[32,2048]{1,0:T(8,128)(2,1)}, bf16[32,2048]{1,0:T(8,128)(2,1)S(1)}, u32[]{:S(2)}, u32[]{:S(2)}) collective-permute-start(bf16[32,2048]{1,0:T(8,128)(2,1)} %get-tuple-element.48), channel_id=1, source_target_pairs={{0,7},{1,6},{2,5},{3,4},{4,3},{5,2},{6,1},{7,0},{8,15},{9,14},{10,... | collective-permute-start | bytes 393224 | tf_op jit(solution)/shard_map/ppermute | solution.py:175
  40.0 2.3 %collective-permute-done.5.refs_8_ = bf16[32,2048]{1,0:T(8,128)(2,1)S(1)} collective-permute-done((bf16[32,2048]{1,0:T(8,128)(2,1)}, bf16[32,2048]{1,0:T(8,128)(2,1)S(1)}, u32[]{:S(2)}, u32[]{:S(2)}) %collective-permute-start.5) | collective-permute-done | bytes 131104 | tf_op jit(solution)/shard_map/ppermute | solution.py:175
  43.8 3.2 %collective-permute-done.7.refs_10_ = bf16[32,2048]{1,0:T(8,128)(2,1)S(1)} collective-permute-done((bf16[32,2048]{1,0:T(8,128)(2,1)}, bf16[32,2048]{1,0:T(8,128)(2,1)S(1)}, u32[]{:S(2)}, u32[]{:S(2)}) %collective-permute-start.7) | collective-permute-done | bytes 131104 | tf_op jit(solution)/shard_map/ppermute | solution.py:175
  47.9 4.7 %shard_map.76 = (bf16[32,2048]{1,0:T(8,128)(2,1)}, bf16[32,2048]{1,0:T(8,128)(2,1)}, bf16[32,2048]{1,0:T(8,128)(2,1)}, bf16[32,2048]{1,0:T(8,128)(2,1)}, bf16[32...) custom-call(bf16[1,2048,512]{2,1,0:T(8,128)(2,1)} %refs_0_.3, ...), custom_call_target="tpu_custom_call" | custom-call | tf_op jit(solution)/shard_map/pallas_call | solution.py:179
  56.3 1.8 %collective-permute-start.13 = (bf16[32,2048]{1,0:T(8,128)(2,1)}, bf16[32,2048]{1,0:T(8,128)(2,1)S(1)}, u32[]{:S(2)}, u32[]{:S(2)}) collective-permute-start(bf16[32,2048]{1,0:T(8,128)(2,1)} %get-tuple-element.55), channel_id=1, source_target_pairs={{0,6},{1,7},{2,4},{3,5},{4,2},{5,3},{6,0},{7,1},{8,14},{9,15},{10,... | collective-permute-start | bytes 393224 | tf_op jit(solution)/shard_map/ppermute | solution.py:175
  58.2 3.4 %collective-permute-start.14 = (bf16[32,2048]{1,0:T(8,128)(2,1)}, bf16[32,2048]{1,0:T(8,128)(2,1)S(1)}, u32[]{:S(2)}, u32[]{:S(2)}) collective-permute-start(bf16[32,2048]{1,0:T(8,128)(2,1)} %get-tuple-element.56), channel_id=1, source_target_pairs={{0,7},{1,6},{2,5},{3,4},{4,3},{5,2},{6,1},{7,0},{8,15},{9,14},{10,... | collective-permute-start | bytes 393224 | tf_op jit(solution)/shard_map/ppermute | solution.py:175
  61.6 2.6 %shard_map.78 = (bf16[32,2048]{1,0:T(8,128)(2,1)}, bf16[32,2048]{1,0:T(8,128)(2,1)}, bf16[32,2048]{1,0:T(8,128)(2,1)}, bf16[32,2048]{1,0:T(8,128)(2,1)}, bf16[32...) custom-call(s32[2]{0:T(128)} %copy-done.6, ...), custom_call_target="tpu_custom_call" | custom-call | tf_op jit(solution)/shard_map/pallas_call | solution.py:157
  64.5 1.9 %collective-permute-start.18 = (bf16[32,2048]{1,0:T(8,128)(2,1)}, bf16[32,2048]{1,0:T(8,128)(2,1)S(1)}, u32[]{:S(2)}, u32[]{:S(2)}) collective-permute-start(bf16[32,2048]{1,0:T(8,128)(2,1)} %get-tuple-element.60), channel_id=1, source_target_pairs={{0,3},{1,2},{2,1},{3,0},{4,7},{5,6},{6,5},{7,4},{8,11},{9,10},{10,... | collective-permute-start | bytes 393224 | tf_op jit(solution)/shard_map/ppermute | solution.py:175
  66.8 2.9 %collective-permute-done.14.refs_7_ = bf16[32,2048]{1,0:T(8,128)(2,1)S(1)} collective-permute-done((bf16[32,2048]{1,0:T(8,128)(2,1)}, bf16[32,2048]{1,0:T(8,128)(2,1)S(1)}, u32[]{:S(2)}, u32[]{:S(2)}) %collective-permute-start.14) | collective-permute-done | bytes 131104 | tf_op jit(solution)/shard_map/ppermute | solution.py:175
  71.9 3.0 %collective-permute-start.15 = (bf16[128,2048]{1,0:T(8,128)(2,1)}, bf16[128,2048]{1,0:T(8,128)(2,1)S(1)}, u32[]{:S(2)}, u32[]{:S(2)}) collective-permute-start(bf16[128,2048]{1,0:T(8,128)(2,1)} %shard_map.77), channel_id=1, source_target_pairs={{0,8},{8,0},{1,9},{9,1},{2,10},{10,2},{3,11},{11,3},{4,12},{12,4},... | collective-permute-start | bytes 1572872 | tf_op jit(solution)/shard_map/ppermute | solution.py:166
  74.9 2.3 %collective-permute-start.20 = (bf16[32,2048]{1,0:T(8,128)(2,1)}, bf16[32,2048]{1,0:T(8,128)(2,1)S(1)}, u32[]{:S(2)}, u32[]{:S(2)}) collective-permute-start(bf16[32,2048]{1,0:T(8,128)(2,1)} %get-tuple-element.62), channel_id=1, source_target_pairs={{0,5},{1,4},{2,7},{3,6},{4,1},{5,0},{6,3},{7,2},{8,13},{9,12},{10,... | collective-permute-start | bytes 393224 | tf_op jit(solution)/shard_map/ppermute | solution.py:175
  77.3 2.0 %collective-permute-start.22 = (bf16[32,2048]{1,0:T(8,128)(2,1)}, bf16[32,2048]{1,0:T(8,128)(2,1)S(1)}, u32[]{:S(2)}, u32[]{:S(2)}) collective-permute-start(bf16[32,2048]{1,0:T(8,128)(2,1)} %get-tuple-element.64), channel_id=1, source_target_pairs={{0,7},{1,6},{2,5},{3,4},{4,3},{5,2},{6,1},{7,0},{8,15},{9,14},{10,... | collective-permute-start | bytes 393224 | tf_op jit(solution)/shard_map/ppermute | solution.py:175
  79.3 10.5 %collective-permute-done.19.refs_7_ = bf16[32,2048]{1,0:T(8,128)(2,1)S(1)} collective-permute-done((bf16[32,2048]{1,0:T(8,128)(2,1)}, bf16[32,2048]{1,0:T(8,128)(2,1)S(1)}, u32[]{:S(2)}, u32[]{:S(2)}) %collective-permute-start.19) | collective-permute-done | bytes 131104 | tf_op jit(solution)/shard_map/ppermute | solution.py:175
  89.8 4.1 %collective-permute-done.20.refs_8_ = bf16[32,2048]{1,0:T(8,128)(2,1)S(1)} collective-permute-done((bf16[32,2048]{1,0:T(8,128)(2,1)}, bf16[32,2048]{1,0:T(8,128)(2,1)S(1)}, u32[]{:S(2)}, u32[]{:S(2)}) %collective-permute-start.20) | collective-permute-done | bytes 131104 | tf_op jit(solution)/shard_map/ppermute | solution.py:175
  93.9 1.4 %collective-permute-done.21.refs_9_ = bf16[32,2048]{1,0:T(8,128)(2,1)S(1)} collective-permute-done((bf16[32,2048]{1,0:T(8,128)(2,1)}, bf16[32,2048]{1,0:T(8,128)(2,1)S(1)}, u32[]{:S(2)}, u32[]{:S(2)}) %collective-permute-start.21) | collective-permute-done | bytes 131104 | tf_op jit(solution)/shard_map/ppermute | solution.py:175
  95.4 3.2 %collective-permute-done.22.refs_10_ = bf16[32,2048]{1,0:T(8,128)(2,1)S(1)} collective-permute-done((bf16[32,2048]{1,0:T(8,128)(2,1)}, bf16[32,2048]{1,0:T(8,128)(2,1)S(1)}, u32[]{:S(2)}, u32[]{:S(2)}) %collective-permute-start.22) | collective-permute-done | bytes 131104 | tf_op jit(solution)/shard_map/ppermute | solution.py:175
  99.5 4.7 %shard_map.79 = (bf16[32,2048]{1,0:T(8,128)(2,1)}, bf16[32,2048]{1,0:T(8,128)(2,1)}, bf16[32,2048]{1,0:T(8,128)(2,1)}, bf16[32,2048]{1,0:T(8,128)(2,1)}, bf16[32...) custom-call(bf16[1,2048,512]{2,1,0:T(8,128)(2,1)} %refs_0_.3, ...), custom_call_target="tpu_custom_call" | custom-call | tf_op jit(solution)/shard_map/pallas_call | solution.py:179
  110.6 2.3 %collective-permute-done.25.refs_3_ = bf16[32,2048]{1,0:T(8,128)(2,1)S(1)} collective-permute-done((bf16[32,2048]{1,0:T(8,128)(2,1)}, bf16[32,2048]{1,0:T(8,128)(2,1)S(1)}, u32[]{:S(2)}, u32[]{:S(2)}) %collective-permute-start.25) | collective-permute-done | bytes 131104 | tf_op jit(solution)/shard_map/ppermute | solution.py:175
  115.3 3.1 %collective-permute-done.28.refs_6_ = bf16[32,2048]{1,0:T(8,128)(2,1)S(1)} collective-permute-done((bf16[32,2048]{1,0:T(8,128)(2,1)}, bf16[32,2048]{1,0:T(8,128)(2,1)S(1)}, u32[]{:S(2)}, u32[]{:S(2)}) %collective-permute-start.28) | collective-permute-done | bytes 131104 | tf_op jit(solution)/shard_map/ppermute | solution.py:175
  118.4 2.8 %collective-permute-done.29.refs_7_ = bf16[32,2048]{1,0:T(8,128)(2,1)S(1)} collective-permute-done((bf16[32,2048]{1,0:T(8,128)(2,1)}, bf16[32,2048]{1,0:T(8,128)(2,1)S(1)}, u32[]{:S(2)}, u32[]{:S(2)}) %collective-permute-start.29) | collective-permute-done | bytes 131104 | tf_op jit(solution)/shard_map/ppermute | solution.py:175
  (67 shorter events, 28.9 us)
Async XLA Ops:
  2.1 26.8 %collective-permute-start = (bf16[128,2176]{1,0:T(8,128)(2,1)}, bf16[128,2176]{1,0:T(8,128)(2,1)S(1)}, u32[]{:S(2)}, u32[]{:S(2)}) collective-permute-start(bf16[128,2176]{1,0:T(8,128)(2,1)} %shard_map.74.block_ref), channel_id=1, source_target_pairs={{0,8},{8,0},{1,9},{9,1},{2,10},{10,2},{3,11},{11,3},{4,12},{12,4},... | collective-permute-start | bytes 1671176 | tf_op jit(solution)/shard_map/ppermute | solution.py:166
  31.7 8.3 %collective-permute-start.3 = (bf16[32,2048]{1,0:T(8,128)(2,1)}, bf16[32,2048]{1,0:T(8,128)(2,1)S(1)}, u32[]{:S(2)}, u32[]{:S(2)}) collective-permute-start(bf16[32,2048]{1,0:T(8,128)(2,1)} %get-tuple-element.44), channel_id=1, source_target_pairs={{0,3},{1,2},{2,1},{3,0},{4,7},{5,6},{6,5},{7,4},{8,11},{9,10},{10,... | collective-permute-start | bytes 393224 | tf_op jit(solution)/shard_map/ppermute | solution.py:175
  33.1 6.9 %collective-permute-start.4 = (bf16[32,2048]{1,0:T(8,128)(2,1)}, bf16[32,2048]{1,0:T(8,128)(2,1)S(1)}, u32[]{:S(2)}, u32[]{:S(2)}) collective-permute-start(bf16[32,2048]{1,0:T(8,128)(2,1)} %get-tuple-element.45), channel_id=1, source_target_pairs={{0,4},{1,5},{2,6},{3,7},{4,0},{5,1},{6,2},{7,3},{8,12},{9,13},{10,... | collective-permute-start | bytes 393224 | tf_op jit(solution)/shard_map/ppermute | solution.py:175
  34.1 8.2 %collective-permute-start.5 = (bf16[32,2048]{1,0:T(8,128)(2,1)}, bf16[32,2048]{1,0:T(8,128)(2,1)S(1)}, u32[]{:S(2)}, u32[]{:S(2)}) collective-permute-start(bf16[32,2048]{1,0:T(8,128)(2,1)} %get-tuple-element.46), channel_id=1, source_target_pairs={{0,5},{1,4},{2,7},{3,6},{4,1},{5,0},{6,3},{7,2},{8,13},{9,12},{10,... | collective-permute-start | bytes 393224 | tf_op jit(solution)/shard_map/ppermute | solution.py:175
  35.0 8.8 %collective-permute-start.6 = (bf16[32,2048]{1,0:T(8,128)(2,1)}, bf16[32,2048]{1,0:T(8,128)(2,1)S(1)}, u32[]{:S(2)}, u32[]{:S(2)}) collective-permute-start(bf16[32,2048]{1,0:T(8,128)(2,1)} %get-tuple-element.47), channel_id=1, source_target_pairs={{0,6},{1,7},{2,4},{3,5},{4,2},{5,3},{6,0},{7,1},{8,14},{9,15},{10,... | collective-permute-start | bytes 393224 | tf_op jit(solution)/shard_map/ppermute | solution.py:175
  36.7 10.2 %collective-permute-start.7 = (bf16[32,2048]{1,0:T(8,128)(2,1)}, bf16[32,2048]{1,0:T(8,128)(2,1)S(1)}, u32[]{:S(2)}, u32[]{:S(2)}) collective-permute-start(bf16[32,2048]{1,0:T(8,128)(2,1)} %get-tuple-element.48), channel_id=1, source_target_pairs={{0,7},{1,6},{2,5},{3,4},{4,3},{5,2},{6,1},{7,0},{8,15},{9,14},{10,... | collective-permute-start | bytes 393224 | tf_op jit(solution)/shard_map/ppermute | solution.py:175
  54.0 10.2 %collective-permute-start.10 = (bf16[32,2048]{1,0:T(8,128)(2,1)}, bf16[32,2048]{1,0:T(8,128)(2,1)S(1)}, u32[]{:S(2)}, u32[]{:S(2)}) collective-permute-start(bf16[32,2048]{1,0:T(8,128)(2,1)} %get-tuple-element.52), channel_id=1, source_target_pairs={{0,3},{1,2},{2,1},{3,0},{4,7},{5,6},{6,5},{7,4},{8,11},{9,10},{10,... | collective-permute-start | bytes 393224 | tf_op jit(solution)/shard_map/ppermute | solution.py:175
  54.8 9.4 %collective-permute-start.11 = (bf16[32,2048]{1,0:T(8,128)(2,1)}, bf16[32,2048]{1,0:T(8,128)(2,1)S(1)}, u32[]{:S(2)}, u32[]{:S(2)}) collective-permute-start(bf16[32,2048]{1,0:T(8,128)(2,1)} %get-tuple-element.53), channel_id=1, source_target_pairs={{0,4},{1,5},{2,6},{3,7},{4,0},{5,1},{6,2},{7,3},{8,12},{9,13},{10,... | collective-permute-start | bytes 393224 | tf_op jit(solution)/shard_map/ppermute | solution.py:175
  55.7 8.7 %collective-permute-start.12 = (bf16[32,2048]{1,0:T(8,128)(2,1)}, bf16[32,2048]{1,0:T(8,128)(2,1)S(1)}, u32[]{:S(2)}, u32[]{:S(2)}) collective-permute-start(bf16[32,2048]{1,0:T(8,128)(2,1)} %get-tuple-element.54), channel_id=1, source_target_pairs={{0,5},{1,4},{2,7},{3,6},{4,1},{5,0},{6,3},{7,2},{8,13},{9,12},{10,... | collective-permute-start | bytes 393224 | tf_op jit(solution)/shard_map/ppermute | solution.py:175
  56.3 10.5 %collective-permute-start.13 = (bf16[32,2048]{1,0:T(8,128)(2,1)}, bf16[32,2048]{1,0:T(8,128)(2,1)S(1)}, u32[]{:S(2)}, u32[]{:S(2)}) collective-permute-start(bf16[32,2048]{1,0:T(8,128)(2,1)} %get-tuple-element.55), channel_id=1, source_target_pairs={{0,6},{1,7},{2,4},{3,5},{4,2},{5,3},{6,0},{7,1},{8,14},{9,15},{10,... | collective-permute-start | bytes 393224 | tf_op jit(solution)/shard_map/ppermute | solution.py:175
  58.2 11.6 %collective-permute-start.14 = (bf16[32,2048]{1,0:T(8,128)(2,1)}, bf16[32,2048]{1,0:T(8,128)(2,1)S(1)}, u32[]{:S(2)}, u32[]{:S(2)}) collective-permute-start(bf16[32,2048]{1,0:T(8,128)(2,1)} %get-tuple-element.56), channel_id=1, source_target_pairs={{0,7},{1,6},{2,5},{3,4},{4,3},{5,2},{6,1},{7,0},{8,15},{9,14},{10,... | collective-permute-start | bytes 393224 | tf_op jit(solution)/shard_map/ppermute | solution.py:175
  64.2 10.8 %collective-permute-start.16 = (bf16[32,2048]{1,0:T(8,128)(2,1)}, bf16[32,2048]{1,0:T(8,128)(2,1)S(1)}, u32[]{:S(2)}, u32[]{:S(2)}) collective-permute-start(bf16[32,2048]{1,0:T(8,128)(2,1)} %get-tuple-element.58), channel_id=1, source_target_pairs={{0,1},{1,0},{2,3},{3,2},{4,5},{5,4},{6,7},{7,6},{8,9},{9,8},{10,11... | collective-permute-start | bytes 393224 | tf_op jit(solution)/shard_map/ppermute | solution.py:175
  64.2 13.1 %collective-permute-start.17 = (bf16[32,2048]{1,0:T(8,128)(2,1)}, bf16[32,2048]{1,0:T(8,128)(2,1)S(1)}, u32[]{:S(2)}, u32[]{:S(2)}) collective-permute-start(bf16[32,2048]{1,0:T(8,128)(2,1)} %get-tuple-element.59), channel_id=1, source_target_pairs={{0,2},{1,3},{2,0},{3,1},{4,6},{5,7},{6,4},{7,5},{8,10},{9,11},{10,... | collective-permute-start | bytes 393224 | tf_op jit(solution)/shard_map/ppermute | solution.py:175
  64.5 12.8 %collective-permute-start.18 = (bf16[32,2048]{1,0:T(8,128)(2,1)}, bf16[32,2048]{1,0:T(8,128)(2,1)S(1)}, u32[]{:S(2)}, u32[]{:S(2)}) collective-permute-start(bf16[32,2048]{1,0:T(8,128)(2,1)} %get-tuple-element.60), channel_id=1, source_target_pairs={{0,3},{1,2},{2,1},{3,0},{4,7},{5,6},{6,5},{7,4},{8,11},{9,10},{10,... | collective-permute-start | bytes 393224 | tf_op jit(solution)/shard_map/ppermute | solution.py:175
  71.9 49.3 %collective-permute-start.15 = (bf16[128,2048]{1,0:T(8,128)(2,1)}, bf16[128,2048]{1,0:T(8,128)(2,1)S(1)}, u32[]{:S(2)}, u32[]{:S(2)}) collective-permute-start(bf16[128,2048]{1,0:T(8,128)(2,1)} %shard_map.77), channel_id=1, source_target_pairs={{0,8},{8,0},{1,9},{9,1},{2,10},{10,2},{3,11},{11,3},{4,12},{12,4},... | collective-permute-start | bytes 1572872 | tf_op jit(solution)/shard_map/ppermute | solution.py:166
  74.9 14.9 %collective-permute-start.19 = (bf16[32,2048]{1,0:T(8,128)(2,1)}, bf16[32,2048]{1,0:T(8,128)(2,1)S(1)}, u32[]{:S(2)}, u32[]{:S(2)}) collective-permute-start(bf16[32,2048]{1,0:T(8,128)(2,1)} %get-tuple-element.61), channel_id=1, source_target_pairs={{0,4},{1,5},{2,6},{3,7},{4,0},{5,1},{6,2},{7,3},{8,12},{9,13},{10,... | collective-permute-start | bytes 393224 | tf_op jit(solution)/shard_map/ppermute | solution.py:175
  74.9 19.0 %collective-permute-start.20 = (bf16[32,2048]{1,0:T(8,128)(2,1)}, bf16[32,2048]{1,0:T(8,128)(2,1)S(1)}, u32[]{:S(2)}, u32[]{:S(2)}) collective-permute-start(bf16[32,2048]{1,0:T(8,128)(2,1)} %get-tuple-element.62), channel_id=1, source_target_pairs={{0,5},{1,4},{2,7},{3,6},{4,1},{5,0},{6,3},{7,2},{8,13},{9,12},{10,... | collective-permute-start | bytes 393224 | tf_op jit(solution)/shard_map/ppermute | solution.py:175
  77.3 18.1 %collective-permute-start.21 = (bf16[32,2048]{1,0:T(8,128)(2,1)}, bf16[32,2048]{1,0:T(8,128)(2,1)S(1)}, u32[]{:S(2)}, u32[]{:S(2)}) collective-permute-start(bf16[32,2048]{1,0:T(8,128)(2,1)} %get-tuple-element.63), channel_id=1, source_target_pairs={{0,6},{1,7},{2,4},{3,5},{4,2},{5,3},{6,0},{7,1},{8,14},{9,15},{10,... | collective-permute-start | bytes 393224 | tf_op jit(solution)/shard_map/ppermute | solution.py:175
  77.3 21.3 %collective-permute-start.22 = (bf16[32,2048]{1,0:T(8,128)(2,1)}, bf16[32,2048]{1,0:T(8,128)(2,1)S(1)}, u32[]{:S(2)}, u32[]{:S(2)}) collective-permute-start(bf16[32,2048]{1,0:T(8,128)(2,1)} %get-tuple-element.64), channel_id=1, source_target_pairs={{0,7},{1,6},{2,5},{3,4},{4,3},{5,2},{6,1},{7,0},{8,15},{9,14},{10,... | collective-permute-start | bytes 393224 | tf_op jit(solution)/shard_map/ppermute | solution.py:175
  105.5 7.3 %collective-permute-start.25 = (bf16[32,2048]{1,0:T(8,128)(2,1)}, bf16[32,2048]{1,0:T(8,128)(2,1)S(1)}, u32[]{:S(2)}, u32[]{:S(2)}) collective-permute-start(bf16[32,2048]{1,0:T(8,128)(2,1)} %get-tuple-element.68), channel_id=1, source_target_pairs={{0,3},{1,2},{2,1},{3,0},{4,7},{5,6},{6,5},{7,4},{8,11},{9,10},{10,... | collective-permute-start | bytes 393224 | tf_op jit(solution)/shard_map/ppermute | solution.py:175
  106.4 8.9 %collective-permute-start.26 = (bf16[32,2048]{1,0:T(8,128)(2,1)}, bf16[32,2048]{1,0:T(8,128)(2,1)S(1)}, u32[]{:S(2)}, u32[]{:S(2)}) collective-permute-start(bf16[32,2048]{1,0:T(8,128)(2,1)} %get-tuple-element.69), channel_id=1, source_target_pairs={{0,4},{1,5},{2,6},{3,7},{4,0},{5,1},{6,2},{7,3},{8,12},{9,13},{10,... | collective-permute-start | bytes 393224 | tf_op jit(solution)/shard_map/ppermute | solution.py:175
  107.1 8.2 %collective-permute-start.27 = (bf16[32,2048]{1,0:T(8,128)(2,1)}, bf16[32,2048]{1,0:T(8,128)(2,1)S(1)}, u32[]{:S(2)}, u32[]{:S(2)}) collective-permute-start(bf16[32,2048]{1,0:T(8,128)(2,1)} %get-tuple-element.70), channel_id=1, source_target_pairs={{0,5},{1,4},{2,7},{3,6},{4,1},{5,0},{6,3},{7,2},{8,13},{9,12},{10,... | collective-permute-start | bytes 393224 | tf_op jit(solution)/shard_map/ppermute | solution.py:175
  109.2 9.2 %collective-permute-start.28 = (bf16[32,2048]{1,0:T(8,128)(2,1)}, bf16[32,2048]{1,0:T(8,128)(2,1)S(1)}, u32[]{:S(2)}, u32[]{:S(2)}) collective-permute-start(bf16[32,2048]{1,0:T(8,128)(2,1)} %get-tuple-element.71), channel_id=1, source_target_pairs={{0,6},{1,7},{2,4},{3,5},{4,2},{5,3},{6,0},{7,1},{8,14},{9,15},{10,... | collective-permute-start | bytes 393224 | tf_op jit(solution)/shard_map/ppermute | solution.py:175
  112.9 8.4 %collective-permute-start.29 = (bf16[32,2048]{1,0:T(8,128)(2,1)}, bf16[32,2048]{1,0:T(8,128)(2,1)S(1)}, u32[]{:S(2)}, u32[]{:S(2)}) collective-permute-start(bf16[32,2048]{1,0:T(8,128)(2,1)} %get-tuple-element.72), channel_id=1, source_target_pairs={{0,7},{1,6},{2,5},{3,4},{4,3},{5,2},{6,1},{7,0},{8,15},{9,14},{10,... | collective-permute-start | bytes 393224 | tf_op jit(solution)/shard_map/ppermute | solution.py:175
  (17 other events, 173.1 us)

commit v3 on v2

--- a/solution.py
+++ b/solution.py
@@ -67,44 +67,33 @@
         ref[...] = value[i * size : (i + 1) * size].astype(ref.dtype)
 
 
-def norm_kernel(hidden_ref, gain_ref, ids_ref, weights_ref, out_ref):
+def normed_of(hidden_ref, gain_ref):
     as_float = hidden_ref[...].astype(jnp.float32)
     scale = lax.rsqrt(jnp.mean(as_float * as_float, axis=-1, keepdims=True) + 1e-06)
-    width = hidden_ref.shape[1]
-    out_ref[:, :width] = (as_float * scale * gain_ref[...]).astype(jnp.bfloat16)
-    facts, left = [ids_ref[...].astype(jnp.float32)], weights_ref[...]
-    for _ in range(3):
-        term = left.astype(jnp.bfloat16).astype(jnp.float32)
-        facts.append(term)
-        left = left - term
-    facts.append(jnp.zeros((LANES - 4 * ids_ref.shape[0], ids_ref.shape[1]), jnp.float32))
-    out_ref[:, width:] = jnp.concatenate(facts, axis=0).T.astype(jnp.bfloat16)
-
-
-def facts_of(block_ref, choose_count):
-    facts = block_ref[:, block_ref.shape[1] - LANES :].astype(jnp.float32).T
-    terms = [facts[(1 + i) * choose_count : (2 + i) * choose_count, :] for i in range(3)]
-    return facts[:choose_count, :].astype(jnp.int32), terms[0] + terms[1] + terms[2]
-
-
-def pack_kernel(layout, keep, place_ref, block_ref, *refs):
-    choose_count, expert_count, count, capacity = layout
-    ids, weights = facts_of(block_ref, choose_count)
-    marks = marks_of(ids, slots_of(ids, expert_count), place_ref[0], place_ref[1], count, capacity)
-    if keep:
-        for k, mark in enumerate(marks):
-            refs[0][k] = as_ones(mark)
-        refs[1][...] = weights
-    rows = block_ref[:, : block_ref.shape[1] - LANES]
-    apart(jnp.dot(as_ones(any_of(marks)), rows, preferred_element_type=jnp.float32), refs[2 * keep :])
-
-
-def mark_kernel(layout, place_ref, ids_ref, out_ref):
-    _, expert_count, count, capacity = layout
+    return (as_float * scale * gain_ref[...]).astype(jnp.bfloat16)
+
+
+def near_kernel(layout, place_ref, hidden_ref, gain_ref, ids_ref, *out_refs):
+    expert_count, count, capacity = layout
     ids = ids_ref[...]
     marks = marks_of(ids, slots_of(ids, expert_count), place_ref[0], place_ref[1], count, capacity)
-    for k, mark in enumerate(marks):
-        out_ref[k] = as_ones(mark)
+    rows = normed_of(hidden_ref, gain_ref)
+    apart(jnp.dot(as_ones(any_of(marks)), rows, preferred_element_type=jnp.float32), out_refs)
+
+
+def mark_kernel(layout, place_ref, *refs):
+    expert_count, count, capacity = layout
+    for ids_ref, out_ref in zip(refs[:2], refs[2:]):
+        ids = ids_ref[...]
+        marks = marks_of(ids, slots_of(ids, expert_count), place_ref[0], place_ref[1], count, capacity)
+        for k, mark in enumerate(marks):
+            out_ref[k] = as_ones(mark)
+
+
+def far_kernel(hidden_ref, gain_ref, marks_ref, *out_refs):
+    chosen = functools.reduce(jnp.add, [marks_ref[k] for k in range(marks_ref.shape[0])])
+    rows = normed_of(hidden_ref, gain_ref)
+    apart(jnp.dot(chosen, rows, preferred_element_type=jnp.float32), out_refs)
 
 
 def expert_kernel(count, *refs):
@@ -133,7 +122,8 @@
     refs[-1][...] = (near + partial_ref[...].astype(jnp.float32)).astype(jnp.bfloat16)
 
 
-LANES = 128
+def in_hbm(value):
+    return pltpu.with_memory_space_constraint(value, pltpu.HBM)
 
 
 def body(hidden_in, expert_ids, route_weights, norm_gain, gate_proj, up_proj, down_proj):
@@ -148,7 +138,7 @@
     turn = lax.axis_index(group) if paired else jnp.int32(0)
     place = jnp.stack([lax.axis_index("eh") * half_count, turn]).astype(jnp.int32)
     ids, weights, gain = expert_ids.T, route_weights.T, norm_gain[None, :]
-    proj = [pltpu.with_memory_space_constraint(w, pltpu.HBM) for w in (gate_proj, up_proj, down_proj)]
+    proj = [in_hbm(w) for w in (gate_proj, up_proj, down_proj)]
 
     def array(*shape):
         return pltpu.HBM(shape, jnp.bfloat16)
@@ -191,21 +181,15 @@
     pieces = half_count if paired else 1
     piece = array(slots // pieces, model_width)
     marks = array(choose_count, slots, token_count)
-    layout = (choose_count, expert_count, half_count, capacity)
-    (block,) = call(
-        norm_kernel, 0, [array(token_count, model_width + LANES)], hidden_in, gain, ids, weights, limit=None
-    )
-    far_block = cross(block)
-    kernel = functools.partial(pack_kernel, layout, False)
-    near = scatter(call(kernel, 1, [piece] * pieces, place, block, limit=None))
-    (near_marks,) = call(functools.partial(mark_kernel, layout), 1, [marks], place, ids)
-    far_marks, far_weights, *far = call(
-        functools.partial(pack_kernel, layout, True),
-        1,
-        [marks, pltpu.HBM((choose_count, token_count), jnp.float32)] + [piece] * pieces,
-        place, far_block,
-    )
-    far = scatter(far)
+    layout = (expert_count, half_count, capacity)
+    far_ids, far_weights = cross(expert_ids).T, cross(route_weights).T
+    far_hidden = cross(hidden_in)
+    kernel = functools.partial(near_kernel, layout)
+    near = call(kernel, 1, [piece] * pieces, place, hidden_in, gain, ids, limit=None)
+    near = scatter(near)
+    kernel = functools.partial(mark_kernel, layout)
+    near_marks, far_marks = call(kernel, 1, [marks, marks], place, ids, far_ids)
+    far = scatter(call(far_kernel, 0, [piece] * pieces, far_hidden, in_hbm(gain), in_hbm(far_marks)))
     near = experts(near)
     far = experts(far)
     far = scatter(far)

time: 126 us -> 126 us (level)
  waiting for transfers between devices: 65.6 us -> 68.7 us
  starting transfers between devices: 33.9 us -> 31.5 us
  Pallas kernels: 20.3 us -> 18.6 us
    ppermute x28, waiting for transfers between devices: 41.2 us -> 45.7 us  [scatter(): lax.ppermute(parts[j], group, [(i, i ^ j) for i in range(half_count)])]
    ppermute x28, starting transfers between devices: 28.6 us -> 26 us  [scatter(): lax.ppermute(parts[j], group, [(i, i ^ j) for i in range(half_count)])]
    pallas_call x6 -> x5, Pallas kernels: 10.8 us -> 9.18 us  [call(): pl.pallas_call(kernel, in_specs=[SMEM] * scalars + [VMEM] * (len(args) -...]
    ppermute x2 -> x4, waiting for transfers between devices: 24.4 us -> 23 us  [cross(): return lax.ppermute(value, 'eh', [(0, 1), (1, 0)])]
    unnamed x22 -> x18, local copies, waits for them, and re-layouts: 4.54 us -> 4.31 us
    ppermute x2 -> x4, starting transfers between devices: 5.31 us -> 5.42 us  [cross(): return lax.ppermute(value, 'eh', [(0, 1), (1, 0)])]
  transfers between devices with their start and end apart: 30 -> 32, of which waited for: 16 -> 19; matrix products, arithmetic and copies ran while one was open for 0% -> 0% of each run, Pallas kernels for 8% -> 8%
where the time goes in v3:
time: 126 us; the launch traced here: 123 us
  waiting for transfers between devices  68.7 us (55%)
  starting transfers between devices  31.5 us (25%)
  Pallas kernels  18.6 us (15%)
  local copies, waits for them, and re-layouts  4.31 us (3%)
    ppermute x28, waiting for transfers between devices, scatter(): lax.ppermute(parts[j], group, [(i, i ^ j) for i in range(half_count)])  45.7 us
    ppermute x28, starting transfers between devices, scatter(): lax.ppermute(parts[j], group, [(i, i ^ j) for i in range(half_count)])  26 us
    ppermute x4, waiting for transfers between devices, cross(): return lax.ppermute(value, 'eh', [(0, 1), (1, 0)])  23 us
    pallas_call x2, Pallas kernels, experts(): pl.pallas_call(functools.partial(expert_kernel, len(rows)), in_specs=[HBM...  9.44 us
    pallas_call x5, Pallas kernels, call(): pl.pallas_call(kernel, in_specs=[SMEM] * scalars + [VMEM] * (len(args) -...  9.18 us
    ppermute x4, starting transfers between devices, cross(): return lax.ppermute(value, 'eh', [(0, 1), (1, 0)])  5.42 us
    unnamed x18, local copies, waits for them, and re-layouts  4.31 us
  transfers between devices with their start and end apart: 32, of which 19 were waited for; matrix products, arithmetic and copies ran while one was open for 0% of the time, Pallas kernels for 8%

profile of v3, /device:TPU:11, one launch (start us, length us, event | category | flops | bytes accessed | tf_op | source)
XLA Modules:
  0.0 123.2 jit_solution(6540498889431533497)
XLA Ops:
  0.0 2.3 %collective-permute-start.2 = (bf16[128,2048]{1,0:T(8,128)(2,1)}, bf16[128,2048]{1,0:T(8,128)(2,1)S(1)}, u32[]{:S(2)}, u32[]{:S(2)}) collective-permute-start(bf16[128,2048]{1,0:T(8,128)(2,1)} %hidden_ref.1), channel_id=1, source_target_pairs={{0,8},{8,0},{1,9},{9,1},{2,10},{10,2},{3,11},{11,3},{4,12},{12,4},... | collective-permute-start | bytes 1572872 | tf_op jit(solution)/shard_map/ppermute | solution.py:156
  2.4 23.0 %collective-permute-done = s32[128,2]{0,1:T(2,128)S(1)} collective-permute-done((s32[128,2]{0,1:T(2,128)}, s32[128,2]{0,1:T(2,128)S(1)}, u32[]{:S(2)}, u32[]{:S(2)}) %collective-permute-start) | collective-permute-done | bytes 1056 | tf_op jit(solution)/shard_map/ppermute | solution.py:156
  27.5 2.5 %shard_map.74 = (bf16[32,2048]{1,0:T(8,128)(2,1)}, bf16[32,2048]{1,0:T(8,128)(2,1)}, bf16[32,2048]{1,0:T(8,128)(2,1)}, bf16[32,2048]{1,0:T(8,128)(2,1)}, bf16[32...) custom-call(bf16[128,2048]{1,0:T(8,128)(2,1)S(1)} %collective-permute-done.2., ...), custom_call_target="tpu_custom_call" | custom-call | tf_op jit(solution)/shard_map/pallas_call | solution.py:147
  35.8 2.2 %collective-permute-start.9 = (bf16[32,2048]{1,0:T(8,128)(2,1)}, bf16[32,2048]{1,0:T(8,128)(2,1)S(1)}, u32[]{:S(2)}, u32[]{:S(2)}) collective-permute-start(bf16[32,2048]{1,0:T(8,128)(2,1)} %get-tuple-element.48), channel_id=1, source_target_pairs={{0,7},{1,6},{2,5},{3,4},{4,3},{5,2},{6,1},{7,0},{8,15},{9,14},{10,... | collective-permute-start | bytes 393224 | tf_op jit(solution)/shard_map/ppermute | solution.py:165
  39.0 2.3 %collective-permute-done.7.refs_8_ = bf16[32,2048]{1,0:T(8,128)(2,1)S(1)} collective-permute-done((bf16[32,2048]{1,0:T(8,128)(2,1)}, bf16[32,2048]{1,0:T(8,128)(2,1)S(1)}, u32[]{:S(2)}, u32[]{:S(2)}) %collective-permute-start.7) | collective-permute-done | bytes 131104 | tf_op jit(solution)/shard_map/ppermute | solution.py:165
  42.8 3.2 %collective-permute-done.9.refs_10_ = bf16[32,2048]{1,0:T(8,128)(2,1)S(1)} collective-permute-done((bf16[32,2048]{1,0:T(8,128)(2,1)}, bf16[32,2048]{1,0:T(8,128)(2,1)S(1)}, u32[]{:S(2)}, u32[]{:S(2)}) %collective-permute-start.9) | collective-permute-done | bytes 131104 | tf_op jit(solution)/shard_map/ppermute | solution.py:165
  46.9 4.7 %shard_map.75 = (bf16[32,2048]{1,0:T(8,128)(2,1)}, bf16[32,2048]{1,0:T(8,128)(2,1)}, bf16[32,2048]{1,0:T(8,128)(2,1)}, bf16[32,2048]{1,0:T(8,128)(2,1)}, bf16[32...) custom-call(bf16[1,2048,512]{2,1,0:T(8,128)(2,1)} %refs_0_.3, ...), custom_call_target="tpu_custom_call" | custom-call | tf_op jit(solution)/shard_map/pallas_call | solution.py:169
  53.0 3.1 %collective-permute-start.1 = (f32[128,2]{0,1:T(2,128)S(1)}, f32[128,2]{0,1:T(2,128)S(1)}, u32[]{:S(2)}, u32[]{:S(2)}) collective-permute-start(f32[128,2]{0,1:T(2,128)S(1)} %copy-done.8), channel_id=1, source_target_pairs={{0,8},{8,0},{1,9},{9,1},{2,10},{10,2},{3,11},{11,3},{4,12},{12,4},... | collective-permute-start | bytes 3080 | tf_op jit(solution)/shard_map/ppermute | solution.py:156
  57.2 1.9 %collective-permute-start.14 = (bf16[32,2048]{1,0:T(8,128)(2,1)}, bf16[32,2048]{1,0:T(8,128)(2,1)S(1)}, u32[]{:S(2)}, u32[]{:S(2)}) collective-permute-start(bf16[32,2048]{1,0:T(8,128)(2,1)} %get-tuple-element.54), channel_id=1, source_target_pairs={{0,5},{1,4},{2,7},{3,6},{4,1},{5,0},{6,3},{7,2},{8,13},{9,12},{10,... | collective-permute-start | bytes 393224 | tf_op jit(solution)/shard_map/ppermute | solution.py:165
  59.9 1.7 %collective-permute-start.16 = (bf16[32,2048]{1,0:T(8,128)(2,1)}, bf16[32,2048]{1,0:T(8,128)(2,1)S(1)}, u32[]{:S(2)}, u32[]{:S(2)}) collective-permute-start(bf16[32,2048]{1,0:T(8,128)(2,1)} %get-tuple-element.56), channel_id=1, source_target_pairs={{0,7},{1,6},{2,5},{3,4},{4,3},{5,2},{6,1},{7,0},{8,15},{9,14},{10,... | collective-permute-start | bytes 393224 | tf_op jit(solution)/shard_map/ppermute | solution.py:165
  61.6 2.6 %shard_map.77 = (bf16[32,2048]{1,0:T(8,128)(2,1)}, bf16[32,2048]{1,0:T(8,128)(2,1)}, bf16[32,2048]{1,0:T(8,128)(2,1)}, bf16[32,2048]{1,0:T(8,128)(2,1)}, bf16[32...) custom-call(s32[2]{0:T(128)} %copy-done.7, ...), custom_call_target="tpu_custom_call" | custom-call | tf_op jit(solution)/shard_map/pallas_call | solution.py:147
  65.7 1.5 %collective-permute-start.20 = (bf16[32,2048]{1,0:T(8,128)(2,1)}, bf16[32,2048]{1,0:T(8,128)(2,1)S(1)}, u32[]{:S(2)}, u32[]{:S(2)}) collective-permute-start(bf16[32,2048]{1,0:T(8,128)(2,1)} %get-tuple-element.60), channel_id=1, source_target_pairs={{0,3},{1,2},{2,1},{3,0},{4,7},{5,6},{6,5},{7,4},{8,11},{9,10},{10,... | collective-permute-start | bytes 393224 | tf_op jit(solution)/shard_map/ppermute | solution.py:165
  67.2 2.2 %collective-permute-done.15.refs_6_ = bf16[32,2048]{1,0:T(8,128)(2,1)S(1)} collective-permute-done((bf16[32,2048]{1,0:T(8,128)(2,1)}, bf16[32,2048]{1,0:T(8,128)(2,1)S(1)}, u32[]{:S(2)}, u32[]{:S(2)}) %collective-permute-start.15) | collective-permute-done | bytes 131104 | tf_op jit(solution)/shard_map/ppermute | solution.py:165
  69.4 2.8 %collective-permute-done.16.refs_7_ = bf16[32,2048]{1,0:T(8,128)(2,1)S(1)} collective-permute-done((bf16[32,2048]{1,0:T(8,128)(2,1)}, bf16[32,2048]{1,0:T(8,128)(2,1)S(1)}, u32[]{:S(2)}, u32[]{:S(2)}) %collective-permute-start.16) | collective-permute-done | bytes 131104 | tf_op jit(solution)/shard_map/ppermute | solution.py:165
  74.6 2.0 %collective-permute-start.22 = (bf16[32,2048]{1,0:T(8,128)(2,1)}, bf16[32,2048]{1,0:T(8,128)(2,1)S(1)}, u32[]{:S(2)}, u32[]{:S(2)}) collective-permute-start(bf16[32,2048]{1,0:T(8,128)(2,1)} %get-tuple-element.62), channel_id=1, source_target_pairs={{0,5},{1,4},{2,7},{3,6},{4,1},{5,0},{6,3},{7,2},{8,13},{9,12},{10,... | collective-permute-start | bytes 393224 | tf_op jit(solution)/shard_map/ppermute | solution.py:165
  78.9 10.3 %collective-permute-done.21.refs_7_ = bf16[32,2048]{1,0:T(8,128)(2,1)S(1)} collective-permute-done((bf16[32,2048]{1,0:T(8,128)(2,1)}, bf16[32,2048]{1,0:T(8,128)(2,1)S(1)}, u32[]{:S(2)}, u32[]{:S(2)}) %collective-permute-start.21) | collective-permute-done | bytes 131104 | tf_op jit(solution)/shard_map/ppermute | solution.py:165
  89.2 4.4 %collective-permute-done.22.refs_8_ = bf16[32,2048]{1,0:T(8,128)(2,1)S(1)} collective-permute-done((bf16[32,2048]{1,0:T(8,128)(2,1)}, bf16[32,2048]{1,0:T(8,128)(2,1)S(1)}, u32[]{:S(2)}, u32[]{:S(2)}) %collective-permute-start.22) | collective-permute-done | bytes 131104 | tf_op jit(solution)/shard_map/ppermute | solution.py:165
  93.6 2.1 %collective-permute-done.23.refs_9_ = bf16[32,2048]{1,0:T(8,128)(2,1)S(1)} collective-permute-done((bf16[32,2048]{1,0:T(8,128)(2,1)}, bf16[32,2048]{1,0:T(8,128)(2,1)S(1)}, u32[]{:S(2)}, u32[]{:S(2)}) %collective-permute-start.23) | collective-permute-done | bytes 131104 | tf_op jit(solution)/shard_map/ppermute | solution.py:165
  95.7 3.4 %collective-permute-done.24.refs_10_ = bf16[32,2048]{1,0:T(8,128)(2,1)S(1)} collective-permute-done((bf16[32,2048]{1,0:T(8,128)(2,1)}, bf16[32,2048]{1,0:T(8,128)(2,1)S(1)}, u32[]{:S(2)}, u32[]{:S(2)}) %collective-permute-start.24) | collective-permute-done | bytes 131104 | tf_op jit(solution)/shard_map/ppermute | solution.py:165
  99.9 4.7 %shard_map.78 = (bf16[32,2048]{1,0:T(8,128)(2,1)}, bf16[32,2048]{1,0:T(8,128)(2,1)}, bf16[32,2048]{1,0:T(8,128)(2,1)}, bf16[32,2048]{1,0:T(8,128)(2,1)}, bf16[32...) custom-call(bf16[1,2048,512]{2,1,0:T(8,128)(2,1)} %refs_0_.3, ...), custom_call_target="tpu_custom_call" | custom-call | tf_op jit(solution)/shard_map/pallas_call | solution.py:169
  105.3 1.6 %collective-permute-start.27 = (bf16[32,2048]{1,0:T(8,128)(2,1)}, bf16[32,2048]{1,0:T(8,128)(2,1)S(1)}, u32[]{:S(2)}, u32[]{:S(2)}) collective-permute-start(bf16[32,2048]{1,0:T(8,128)(2,1)} %get-tuple-element.68), channel_id=1, source_target_pairs={{0,3},{1,2},{2,1},{3,0},{4,7},{5,6},{6,5},{7,4},{8,11},{9,10},{10,... | collective-permute-start | bytes 393224 | tf_op jit(solution)/shard_map/ppermute | solution.py:165
  110.0 3.4 %collective-permute-done.27.refs_3_ = bf16[32,2048]{1,0:T(8,128)(2,1)S(1)} collective-permute-done((bf16[32,2048]{1,0:T(8,128)(2,1)}, bf16[32,2048]{1,0:T(8,128)(2,1)S(1)}, u32[]{:S(2)}, u32[]{:S(2)}) %collective-permute-start.27) | collective-permute-done | bytes 131104 | tf_op jit(solution)/shard_map/ppermute | solution.py:165
  115.4 2.5 %collective-permute-done.30.refs_6_ = bf16[32,2048]{1,0:T(8,128)(2,1)S(1)} collective-permute-done((bf16[32,2048]{1,0:T(8,128)(2,1)}, bf16[32,2048]{1,0:T(8,128)(2,1)S(1)}, u32[]{:S(2)}, u32[]{:S(2)}) %collective-permute-start.30) | collective-permute-done | bytes 131104 | tf_op jit(solution)/shard_map/ppermute | solution.py:165
  117.8 3.1 %collective-permute-done.31.refs_7_ = bf16[32,2048]{1,0:T(8,128)(2,1)S(1)} collective-permute-done((bf16[32,2048]{1,0:T(8,128)(2,1)}, bf16[32,2048]{1,0:T(8,128)(2,1)S(1)}, u32[]{:S(2)}, u32[]{:S(2)}) %collective-permute-start.31) | collective-permute-done | bytes 131104 | tf_op jit(solution)/shard_map/ppermute | solution.py:165
  (66 shorter events, 29.9 us)
Async XLA Ops:
  0.0 27.5 %collective-permute-start.2 = (bf16[128,2048]{1,0:T(8,128)(2,1)}, bf16[128,2048]{1,0:T(8,128)(2,1)S(1)}, u32[]{:S(2)}, u32[]{:S(2)}) collective-permute-start(bf16[128,2048]{1,0:T(8,128)(2,1)} %hidden_ref.1), channel_id=1, source_target_pairs={{0,8},{8,0},{1,9},{9,1},{2,10},{10,2},{3,11},{11,3},{4,12},{12,4},... | collective-permute-start | bytes 1572872 | tf_op jit(solution)/shard_map/ppermute | solution.py:156
  2.3 23.1 %collective-permute-start = (s32[128,2]{0,1:T(2,128)}, s32[128,2]{0,1:T(2,128)S(1)}, u32[]{:S(2)}, u32[]{:S(2)}) collective-permute-start(s32[128,2]{0,1:T(2,128)} %param.8), channel_id=1, source_target_pairs={{0,8},{8,0},{1,9},{9,1},{2,10},{10,2},{3,11},{11,3},{4,12},{12,4},... | collective-permute-start | bytes 3080 | tf_op jit(solution)/shard_map/ppermute | solution.py:156
  30.8 8.3 %collective-permute-start.5 = (bf16[32,2048]{1,0:T(8,128)(2,1)}, bf16[32,2048]{1,0:T(8,128)(2,1)S(1)}, u32[]{:S(2)}, u32[]{:S(2)}) collective-permute-start(bf16[32,2048]{1,0:T(8,128)(2,1)} %get-tuple-element.44), channel_id=1, source_target_pairs={{0,3},{1,2},{2,1},{3,0},{4,7},{5,6},{6,5},{7,4},{8,11},{9,10},{10,... | collective-permute-start | bytes 393224 | tf_op jit(solution)/shard_map/ppermute | solution.py:165
  33.2 8.2 %collective-permute-start.7 = (bf16[32,2048]{1,0:T(8,128)(2,1)}, bf16[32,2048]{1,0:T(8,128)(2,1)S(1)}, u32[]{:S(2)}, u32[]{:S(2)}) collective-permute-start(bf16[32,2048]{1,0:T(8,128)(2,1)} %get-tuple-element.46), channel_id=1, source_target_pairs={{0,5},{1,4},{2,7},{3,6},{4,1},{5,0},{6,3},{7,2},{8,13},{9,12},{10,... | collective-permute-start | bytes 393224 | tf_op jit(solution)/shard_map/ppermute | solution.py:165
  34.0 8.8 %collective-permute-start.8 = (bf16[32,2048]{1,0:T(8,128)(2,1)}, bf16[32,2048]{1,0:T(8,128)(2,1)S(1)}, u32[]{:S(2)}, u32[]{:S(2)}) collective-permute-start(bf16[32,2048]{1,0:T(8,128)(2,1)} %get-tuple-element.47), channel_id=1, source_target_pairs={{0,6},{1,7},{2,4},{3,5},{4,2},{5,3},{6,0},{7,1},{8,14},{9,15},{10,... | collective-permute-start | bytes 393224 | tf_op jit(solution)/shard_map/ppermute | solution.py:165
  35.8 10.2 %collective-permute-start.9 = (bf16[32,2048]{1,0:T(8,128)(2,1)}, bf16[32,2048]{1,0:T(8,128)(2,1)S(1)}, u32[]{:S(2)}, u32[]{:S(2)}) collective-permute-start(bf16[32,2048]{1,0:T(8,128)(2,1)} %get-tuple-element.48), channel_id=1, source_target_pairs={{0,7},{1,6},{2,5},{3,4},{4,3},{5,2},{6,1},{7,0},{8,15},{9,14},{10,... | collective-permute-start | bytes 393224 | tf_op jit(solution)/shard_map/ppermute | solution.py:165
  51.7 8.2 %collective-permute-start.11 = (bf16[32,2048]{1,0:T(8,128)(2,1)}, bf16[32,2048]{1,0:T(8,128)(2,1)S(1)}, u32[]{:S(2)}, u32[]{:S(2)}) collective-permute-start(bf16[32,2048]{1,0:T(8,128)(2,1)} %get-tuple-element.51), channel_id=1, source_target_pairs={{0,2},{1,3},{2,0},{3,1},{4,6},{5,7},{6,4},{7,5},{8,10},{9,11},{10,... | collective-permute-start | bytes 393224 | tf_op jit(solution)/shard_map/ppermute | solution.py:165
  56.0 8.1 %collective-permute-start.12 = (bf16[32,2048]{1,0:T(8,128)(2,1)}, bf16[32,2048]{1,0:T(8,128)(2,1)S(1)}, u32[]{:S(2)}, u32[]{:S(2)}) collective-permute-start(bf16[32,2048]{1,0:T(8,128)(2,1)} %get-tuple-element.52), channel_id=1, source_target_pairs={{0,3},{1,2},{2,1},{3,0},{4,7},{5,6},{6,5},{7,4},{8,11},{9,10},{10,... | collective-permute-start | bytes 393224 | tf_op jit(solution)/shard_map/ppermute | solution.py:165
  57.2 8.6 %collective-permute-start.14 = (bf16[32,2048]{1,0:T(8,128)(2,1)}, bf16[32,2048]{1,0:T(8,128)(2,1)S(1)}, u32[]{:S(2)}, u32[]{:S(2)}) collective-permute-start(bf16[32,2048]{1,0:T(8,128)(2,1)} %get-tuple-element.54), channel_id=1, source_target_pairs={{0,5},{1,4},{2,7},{3,6},{4,1},{5,0},{6,3},{7,2},{8,13},{9,12},{10,... | collective-permute-start | bytes 393224 | tf_op jit(solution)/shard_map/ppermute | solution.py:165
  59.1 10.4 %collective-permute-start.15 = (bf16[32,2048]{1,0:T(8,128)(2,1)}, bf16[32,2048]{1,0:T(8,128)(2,1)S(1)}, u32[]{:S(2)}, u32[]{:S(2)}) collective-permute-start(bf16[32,2048]{1,0:T(8,128)(2,1)} %get-tuple-element.55), channel_id=1, source_target_pairs={{0,6},{1,7},{2,4},{3,5},{4,2},{5,3},{6,0},{7,1},{8,14},{9,15},{10,... | collective-permute-start | bytes 393224 | tf_op jit(solution)/shard_map/ppermute | solution.py:165
  59.9 12.3 %collective-permute-start.16 = (bf16[32,2048]{1,0:T(8,128)(2,1)}, bf16[32,2048]{1,0:T(8,128)(2,1)S(1)}, u32[]{:S(2)}, u32[]{:S(2)}) collective-permute-start(bf16[32,2048]{1,0:T(8,128)(2,1)} %get-tuple-element.56), channel_id=1, source_target_pairs={{0,7},{1,6},{2,5},{3,4},{4,3},{5,2},{6,1},{7,0},{8,15},{9,14},{10,... | collective-permute-start | bytes 393224 | tf_op jit(solution)/shard_map/ppermute | solution.py:165
  64.2 10.5 %collective-permute-start.18 = (bf16[32,2048]{1,0:T(8,128)(2,1)}, bf16[32,2048]{1,0:T(8,128)(2,1)S(1)}, u32[]{:S(2)}, u32[]{:S(2)}) collective-permute-start(bf16[32,2048]{1,0:T(8,128)(2,1)} %get-tuple-element.58), channel_id=1, source_target_pairs={{0,1},{1,0},{2,3},{3,2},{4,5},{5,4},{6,7},{7,6},{8,9},{9,8},{10,11... | collective-permute-start | bytes 393224 | tf_op jit(solution)/shard_map/ppermute | solution.py:165
  64.5 12.1 %collective-permute-start.19 = (bf16[32,2048]{1,0:T(8,128)(2,1)}, bf16[32,2048]{1,0:T(8,128)(2,1)S(1)}, u32[]{:S(2)}, u32[]{:S(2)}) collective-permute-start(bf16[32,2048]{1,0:T(8,128)(2,1)} %get-tuple-element.59), channel_id=1, source_target_pairs={{0,2},{1,3},{2,0},{3,1},{4,6},{5,7},{6,4},{7,5},{8,10},{9,11},{10,... | collective-permute-start | bytes 393224 | tf_op jit(solution)/shard_map/ppermute | solution.py:165
  65.7 12.1 %collective-permute-start.20 = (bf16[32,2048]{1,0:T(8,128)(2,1)}, bf16[32,2048]{1,0:T(8,128)(2,1)S(1)}, u32[]{:S(2)}, u32[]{:S(2)}) collective-permute-start(bf16[32,2048]{1,0:T(8,128)(2,1)} %get-tuple-element.60), channel_id=1, source_target_pairs={{0,3},{1,2},{2,1},{3,0},{4,7},{5,6},{6,5},{7,4},{8,11},{9,10},{10,... | collective-permute-start | bytes 393224 | tf_op jit(solution)/shard_map/ppermute | solution.py:165
  74.5 46.4 %collective-permute-start.17 = (bf16[128,2048]{1,0:T(8,128)(2,1)}, bf16[128,2048]{1,0:T(8,128)(2,1)S(1)}, u32[]{:S(2)}, u32[]{:S(2)}) collective-permute-start(bf16[128,2048]{1,0:T(8,128)(2,1)} %shard_map.76), channel_id=1, source_target_pairs={{0,8},{8,0},{1,9},{9,1},{2,10},{10,2},{3,11},{11,3},{4,12},{12,4},... | collective-permute-start | bytes 1572872 | tf_op jit(solution)/shard_map/ppermute | solution.py:156
  74.5 14.7 %collective-permute-start.21 = (bf16[32,2048]{1,0:T(8,128)(2,1)}, bf16[32,2048]{1,0:T(8,128)(2,1)S(1)}, u32[]{:S(2)}, u32[]{:S(2)}) collective-permute-start(bf16[32,2048]{1,0:T(8,128)(2,1)} %get-tuple-element.61), channel_id=1, source_target_pairs={{0,4},{1,5},{2,6},{3,7},{4,0},{5,1},{6,2},{7,3},{8,12},{9,13},{10,... | collective-permute-start | bytes 393224 | tf_op jit(solution)/shard_map/ppermute | solution.py:165
  74.6 19.0 %collective-permute-start.22 = (bf16[32,2048]{1,0:T(8,128)(2,1)}, bf16[32,2048]{1,0:T(8,128)(2,1)S(1)}, u32[]{:S(2)}, u32[]{:S(2)}) collective-permute-start(bf16[32,2048]{1,0:T(8,128)(2,1)} %get-tuple-element.62), channel_id=1, source_target_pairs={{0,5},{1,4},{2,7},{3,6},{4,1},{5,0},{6,3},{7,2},{8,13},{9,12},{10,... | collective-permute-start | bytes 393224 | tf_op jit(solution)/shard_map/ppermute | solution.py:165
  76.6 19.1 %collective-permute-start.23 = (bf16[32,2048]{1,0:T(8,128)(2,1)}, bf16[32,2048]{1,0:T(8,128)(2,1)S(1)}, u32[]{:S(2)}, u32[]{:S(2)}) collective-permute-start(bf16[32,2048]{1,0:T(8,128)(2,1)} %get-tuple-element.63), channel_id=1, source_target_pairs={{0,6},{1,7},{2,4},{3,5},{4,2},{5,3},{6,0},{7,1},{8,14},{9,15},{10,... | collective-permute-start | bytes 393224 | tf_op jit(solution)/shard_map/ppermute | solution.py:165
  77.8 21.3 %collective-permute-start.24 = (bf16[32,2048]{1,0:T(8,128)(2,1)}, bf16[32,2048]{1,0:T(8,128)(2,1)S(1)}, u32[]{:S(2)}, u32[]{:S(2)}) collective-permute-start(bf16[32,2048]{1,0:T(8,128)(2,1)} %get-tuple-element.64), channel_id=1, source_target_pairs={{0,7},{1,6},{2,5},{3,4},{4,3},{5,2},{6,1},{7,0},{8,15},{9,14},{10,... | collective-permute-start | bytes 393224 | tf_op jit(solution)/shard_map/ppermute | solution.py:165
  105.3 8.1 %collective-permute-start.27 = (bf16[32,2048]{1,0:T(8,128)(2,1)}, bf16[32,2048]{1,0:T(8,128)(2,1)S(1)}, u32[]{:S(2)}, u32[]{:S(2)}) collective-permute-start(bf16[32,2048]{1,0:T(8,128)(2,1)} %get-tuple-element.68), channel_id=1, source_target_pairs={{0,3},{1,2},{2,1},{3,0},{4,7},{5,6},{6,5},{7,4},{8,11},{9,10},{10,... | collective-permute-start | bytes 393224 | tf_op jit(solution)/shard_map/ppermute | solution.py:165
  106.9 7.5 %collective-permute-start.28 = (bf16[32,2048]{1,0:T(8,128)(2,1)}, bf16[32,2048]{1,0:T(8,128)(2,1)S(1)}, u32[]{:S(2)}, u32[]{:S(2)}) collective-permute-start(bf16[32,2048]{1,0:T(8,128)(2,1)} %get-tuple-element.69), channel_id=1, source_target_pairs={{0,4},{1,5},{2,6},{3,7},{4,0},{5,1},{6,2},{7,3},{8,12},{9,13},{10,... | collective-permute-start | bytes 393224 | tf_op jit(solution)/shard_map/ppermute | solution.py:165
  106.9 8.5 %collective-permute-start.29 = (bf16[32,2048]{1,0:T(8,128)(2,1)}, bf16[32,2048]{1,0:T(8,128)(2,1)S(1)}, u32[]{:S(2)}, u32[]{:S(2)}) collective-permute-start(bf16[32,2048]{1,0:T(8,128)(2,1)} %get-tuple-element.70), channel_id=1, source_target_pairs={{0,5},{1,4},{2,7},{3,6},{4,1},{5,0},{6,3},{7,2},{8,13},{9,12},{10,... | collective-permute-start | bytes 393224 | tf_op jit(solution)/shard_map/ppermute | solution.py:165
  109.7 8.2 %collective-permute-start.30 = (bf16[32,2048]{1,0:T(8,128)(2,1)}, bf16[32,2048]{1,0:T(8,128)(2,1)S(1)}, u32[]{:S(2)}, u32[]{:S(2)}) collective-permute-start(bf16[32,2048]{1,0:T(8,128)(2,1)} %get-tuple-element.71), channel_id=1, source_target_pairs={{0,6},{1,7},{2,4},{3,5},{4,2},{5,3},{6,0},{7,1},{8,14},{9,15},{10,... | collective-permute-start | bytes 393224 | tf_op jit(solution)/shard_map/ppermute | solution.py:165
  113.4 7.5 %collective-permute-start.31 = (bf16[32,2048]{1,0:T(8,128)(2,1)}, bf16[32,2048]{1,0:T(8,128)(2,1)S(1)}, u32[]{:S(2)}, u32[]{:S(2)}) collective-permute-start(bf16[32,2048]{1,0:T(8,128)(2,1)} %get-tuple-element.72), channel_id=1, source_target_pairs={{0,7},{1,6},{2,5},{3,4},{4,3},{5,2},{6,1},{7,0},{8,15},{9,14},{10,... | collective-permute-start | bytes 393224 | tf_op jit(solution)/shard_map/ppermute | solution.py:165
  (17 other events, 148.1 us)

commit v4 on v3

--- a/solution.py
+++ b/solution.py
@@ -81,19 +81,20 @@
     apart(jnp.dot(as_ones(any_of(marks)), rows, preferred_element_type=jnp.float32), out_refs)
 
 
-def mark_kernel(layout, place_ref, *refs):
+def mark_kernel(layout, place_ref, gain_ref, near_ids_ref, far_ids_ref, near_ref, far_ref, chosen_ref, held_ref):
     expert_count, count, capacity = layout
-    for ids_ref, out_ref in zip(refs[:2], refs[2:]):
+    for ids_ref, out_ref in ((near_ids_ref, near_ref), (far_ids_ref, far_ref)):
         ids = ids_ref[...]
         marks = marks_of(ids, slots_of(ids, expert_count), place_ref[0], place_ref[1], count, capacity)
         for k, mark in enumerate(marks):
             out_ref[k] = as_ones(mark)
-
-
-def far_kernel(hidden_ref, gain_ref, marks_ref, *out_refs):
-    chosen = functools.reduce(jnp.add, [marks_ref[k] for k in range(marks_ref.shape[0])])
+    chosen_ref[...] = as_ones(any_of(marks))
+    held_ref[...] = gain_ref[...]
+
+
+def far_kernel(hidden_ref, gain_ref, chosen_ref, *out_refs):
     rows = normed_of(hidden_ref, gain_ref)
-    apart(jnp.dot(chosen, rows, preferred_element_type=jnp.float32), out_refs)
+    apart(jnp.dot(chosen_ref[...], rows, preferred_element_type=jnp.float32), out_refs)
 
 
 def expert_kernel(count, *refs):
@@ -165,12 +166,13 @@
             moved.append(lax.ppermute(parts[j], group, [(i, i ^ j) for i in range(half_count)]))
         return moved
 
-    def experts(rows):
+    def experts(name, rows):
+        own = [pltpu.VMEM(rows[0].shape, jnp.bfloat16)] if paired and name == "far_experts" else []
         return pl.pallas_call(
             functools.partial(expert_kernel, len(rows)),
             in_specs=[HBM] * 3 + [VMEM] * len(rows),
             out_specs=[VMEM] * len(rows),
-            out_shape=[array(*r.shape) for r in rows],
+            out_shape=[*own, *[array(*r.shape) for r in rows[len(own) :]]],
             scratch_shapes=[
                 *[pltpu.VMEM(w.shape[1:], w.dtype) for w in proj],
                 pltpu.SemaphoreType.DMA((3,)),
@@ -188,10 +190,11 @@
     near = call(kernel, 1, [piece] * pieces, place, hidden_in, gain, ids, limit=None)
     near = scatter(near)
     kernel = functools.partial(mark_kernel, layout)
-    near_marks, far_marks = call(kernel, 1, [marks, marks], place, ids, far_ids)
-    far = scatter(call(far_kernel, 0, [piece] * pieces, far_hidden, in_hbm(gain), in_hbm(far_marks)))
-    near = experts(near)
-    far = experts(far)
+    held = [pltpu.VMEM((slots, token_count), jnp.bfloat16), pltpu.VMEM(gain.shape, gain.dtype)]
+    near_marks, far_marks, chosen, gain = call(kernel, 1, [marks, marks, *held], place, gain, ids, far_ids)
+    far = scatter(call(far_kernel, 0, [piece] * pieces, far_hidden, gain, chosen))
+    near = experts("near_experts", near)
+    far = experts("far_experts", far)
     far = scatter(far)
     near = scatter(near)
     (partial,) = call(partial_kernel, 0, [array(token_count, model_width)], far_weights, far_marks, *far)

time: 126 us -> 124 us (0.984)
  no operation moved by 1% of the time
where the time goes in v4:
time: 124 us; the launch traced here: 122 us
  waiting for transfers between devices  69.5 us (56%)
  starting transfers between devices  30.6 us (25%)
  Pallas kernels  17.7 us (14%)
  local copies, waits for them, and re-layouts  4.1 us (3%)
    ppermute x28, waiting for transfers between devices, scatter(): lax.ppermute(parts[j], group, [(i, i ^ j) for i in range(half_count)])  46.5 us
    ppermute x28, starting transfers between devices, scatter(): lax.ppermute(parts[j], group, [(i, i ^ j) for i in range(half_count)])  25.2 us
    ppermute x4, waiting for transfers between devices, cross(): return lax.ppermute(value, 'eh', [(0, 1), (1, 0)])  23 us
    pallas_call x2, Pallas kernels, experts(): pl.pallas_call(functools.partial(expert_kernel, len(rows)), in_specs=[HBM...  9.4 us
    pallas_call x5, Pallas kernels, call(): pl.pallas_call(kernel, in_specs=[SMEM] * scalars + [VMEM] * (len(args) -...  8.26 us
    ppermute x4, starting transfers between devices, cross(): return lax.ppermute(value, 'eh', [(0, 1), (1, 0)])  5.41 us
    unnamed x18, local copies, waits for them, and re-layouts  4.1 us
  transfers between devices with their start and end apart: 32, of which 19 were waited for; matrix products, arithmetic and copies ran while one was open for 0% of the time, Pallas kernels for 8%

profile of v4, /device:TPU:11, one launch (start us, length us, event | category | flops | bytes accessed | tf_op | source)
XLA Modules:
  0.0 122.0 jit_solution(15127834513811056378)
XLA Ops:
  0.0 2.3 %collective-permute-start.2 = (bf16[128,2048]{1,0:T(8,128)(2,1)}, bf16[128,2048]{1,0:T(8,128)(2,1)S(1)}, u32[]{:S(2)}, u32[]{:S(2)}) collective-permute-start(bf16[128,2048]{1,0:T(8,128)(2,1)} %hidden_ref.1), channel_id=1, source_target_pairs={{0,8},{8,0},{1,9},{9,1},{2,10},{10,2},{3,11},{11,3},{4,12},{12,4},... | collective-permute-start | bytes 1572872 | tf_op jit(solution)/shard_map/ppermute | solution.py:157
  2.4 23.0 %collective-permute-done = s32[128,2]{0,1:T(2,128)S(1)} collective-permute-done((s32[128,2]{0,1:T(2,128)}, s32[128,2]{0,1:T(2,128)S(1)}, u32[]{:S(2)}, u32[]{:S(2)}) %collective-permute-start) | collective-permute-done | bytes 1056 | tf_op jit(solution)/shard_map/ppermute | solution.py:157
  28.2 1.5 %shard_map.74 = (bf16[32,2048]{1,0:T(8,128)(2,1)}, bf16[32,2048]{1,0:T(8,128)(2,1)}, bf16[32,2048]{1,0:T(8,128)(2,1)}, bf16[32,2048]{1,0:T(8,128)(2,1)}, bf16[32...) custom-call(bf16[128,2048]{1,0:T(8,128)(2,1)S(1)} %collective-permute-done.2., ...), custom_call_target="tpu_custom_call" | custom-call | tf_op jit(solution)/shard_map/pallas_call | solution.py:148
  35.6 2.2 %collective-permute-start.9 = (bf16[32,2048]{1,0:T(8,128)(2,1)}, bf16[32,2048]{1,0:T(8,128)(2,1)S(1)}, u32[]{:S(2)}, u32[]{:S(2)}) collective-permute-start(bf16[32,2048]{1,0:T(8,128)(2,1)} %get-tuple-element.52), channel_id=1, source_target_pairs={{0,7},{1,6},{2,5},{3,4},{4,3},{5,2},{6,1},{7,0},{8,15},{9,14},{10,... | collective-permute-start | bytes 393224 | tf_op jit(solution)/shard_map/ppermute | solution.py:166
  38.8 2.3 %collective-permute-done.7.refs_8_ = bf16[32,2048]{1,0:T(8,128)(2,1)S(1)} collective-permute-done((bf16[32,2048]{1,0:T(8,128)(2,1)}, bf16[32,2048]{1,0:T(8,128)(2,1)S(1)}, u32[]{:S(2)}, u32[]{:S(2)}) %collective-permute-start.7) | collective-permute-done | bytes 131104 | tf_op jit(solution)/shard_map/ppermute | solution.py:166
  42.6 3.2 %collective-permute-done.9.refs_10_ = bf16[32,2048]{1,0:T(8,128)(2,1)S(1)} collective-permute-done((bf16[32,2048]{1,0:T(8,128)(2,1)}, bf16[32,2048]{1,0:T(8,128)(2,1)S(1)}, u32[]{:S(2)}, u32[]{:S(2)}) %collective-permute-start.9) | collective-permute-done | bytes 131104 | tf_op jit(solution)/shard_map/ppermute | solution.py:166
  46.7 4.7 %shard_map.75 = (bf16[32,2048]{1,0:T(8,128)(2,1)S(1)}, bf16[32,2048]{1,0:T(8,128)(2,1)}, bf16[32,2048]{1,0:T(8,128)(2,1)}, bf16[32,2048]{1,0:T(8,128)(2,1)}, bf1...) custom-call(bf16[1,2048,512]{2,1,0:T(8,128)(2,1)} %refs_0_.3, ...), custom_call_target="tpu_custom_call" | custom-call | tf_op jit(solution)/shard_map/pallas_call | solution.py:171
  52.7 3.0 %collective-permute-start.1 = (f32[128,2]{0,1:T(2,128)S(1)}, f32[128,2]{0,1:T(2,128)S(1)}, u32[]{:S(2)}, u32[]{:S(2)}) collective-permute-start(f32[128,2]{0,1:T(2,128)S(1)} %copy-done.8), channel_id=1, source_target_pairs={{0,8},{8,0},{1,9},{9,1},{2,10},{10,2},{3,11},{11,3},{4,12},{12,4},... | collective-permute-start | bytes 3080 | tf_op jit(solution)/shard_map/ppermute | solution.py:157
  56.9 1.9 %collective-permute-start.14 = (bf16[32,2048]{1,0:T(8,128)(2,1)}, bf16[32,2048]{1,0:T(8,128)(2,1)S(1)}, u32[]{:S(2)}, u32[]{:S(2)}) collective-permute-start(bf16[32,2048]{1,0:T(8,128)(2,1)} %get-tuple-element.58), channel_id=1, source_target_pairs={{0,5},{1,4},{2,7},{3,6},{4,1},{5,0},{6,3},{7,2},{8,13},{9,12},{10,... | collective-permute-start | bytes 393224 | tf_op jit(solution)/shard_map/ppermute | solution.py:166
  59.6 1.7 %collective-permute-start.16 = (bf16[32,2048]{1,0:T(8,128)(2,1)}, bf16[32,2048]{1,0:T(8,128)(2,1)S(1)}, u32[]{:S(2)}, u32[]{:S(2)}) collective-permute-start(bf16[32,2048]{1,0:T(8,128)(2,1)} %get-tuple-element.60), channel_id=1, source_target_pairs={{0,7},{1,6},{2,5},{3,4},{4,3},{5,2},{6,1},{7,0},{8,15},{9,14},{10,... | collective-permute-start | bytes 393224 | tf_op jit(solution)/shard_map/ppermute | solution.py:166
  61.3 2.6 %shard_map.77 = (bf16[32,2048]{1,0:T(8,128)(2,1)}, bf16[32,2048]{1,0:T(8,128)(2,1)}, bf16[32,2048]{1,0:T(8,128)(2,1)}, bf16[32,2048]{1,0:T(8,128)(2,1)}, bf16[32...) custom-call(s32[2]{0:T(128)} %copy-done.7, ...), custom_call_target="tpu_custom_call" | custom-call | tf_op jit(solution)/shard_map/pallas_call | solution.py:148
  65.5 1.5 %collective-permute-start.20 = (bf16[32,2048]{1,0:T(8,128)(2,1)}, bf16[32,2048]{1,0:T(8,128)(2,1)S(1)}, u32[]{:S(2)}, u32[]{:S(2)}) collective-permute-start(bf16[32,2048]{1,0:T(8,128)(2,1)} %get-tuple-element.64), channel_id=1, source_target_pairs={{0,3},{1,2},{2,1},{3,0},{4,7},{5,6},{6,5},{7,4},{8,11},{9,10},{10,... | collective-permute-start | bytes 393224 | tf_op jit(solution)/shard_map/ppermute | solution.py:166
  66.9 2.2 %collective-permute-done.15.refs_6_ = bf16[32,2048]{1,0:T(8,128)(2,1)S(1)} collective-permute-done((bf16[32,2048]{1,0:T(8,128)(2,1)}, bf16[32,2048]{1,0:T(8,128)(2,1)S(1)}, u32[]{:S(2)}, u32[]{:S(2)}) %collective-permute-start.15) | collective-permute-done | bytes 131104 | tf_op jit(solution)/shard_map/ppermute | solution.py:166
  69.2 2.8 %collective-permute-done.16.refs_7_ = bf16[32,2048]{1,0:T(8,128)(2,1)S(1)} collective-permute-done((bf16[32,2048]{1,0:T(8,128)(2,1)}, bf16[32,2048]{1,0:T(8,128)(2,1)S(1)}, u32[]{:S(2)}, u32[]{:S(2)}) %collective-permute-start.16) | collective-permute-done | bytes 131104 | tf_op jit(solution)/shard_map/ppermute | solution.py:166
  73.4 2.0 %collective-permute-start.22 = (bf16[32,2048]{1,0:T(8,128)(2,1)}, bf16[32,2048]{1,0:T(8,128)(2,1)S(1)}, u32[]{:S(2)}, u32[]{:S(2)}) collective-permute-start(bf16[32,2048]{1,0:T(8,128)(2,1)} %get-tuple-element.66), channel_id=1, source_target_pairs={{0,5},{1,4},{2,7},{3,6},{4,1},{5,0},{6,3},{7,2},{8,13},{9,12},{10,... | collective-permute-start | bytes 393224 | tf_op jit(solution)/shard_map/ppermute | solution.py:166
  77.8 10.2 %collective-permute-done.21.refs_7_ = bf16[32,2048]{1,0:T(8,128)(2,1)S(1)} collective-permute-done((bf16[32,2048]{1,0:T(8,128)(2,1)}, bf16[32,2048]{1,0:T(8,128)(2,1)S(1)}, u32[]{:S(2)}, u32[]{:S(2)}) %collective-permute-start.21) | collective-permute-done | bytes 131104 | tf_op jit(solution)/shard_map/ppermute | solution.py:166
  88.0 4.5 %collective-permute-done.22.refs_8_ = bf16[32,2048]{1,0:T(8,128)(2,1)S(1)} collective-permute-done((bf16[32,2048]{1,0:T(8,128)(2,1)}, bf16[32,2048]{1,0:T(8,128)(2,1)S(1)}, u32[]{:S(2)}, u32[]{:S(2)}) %collective-permute-start.22) | collective-permute-done | bytes 131104 | tf_op jit(solution)/shard_map/ppermute | solution.py:166
  92.5 2.1 %collective-permute-done.23.refs_9_ = bf16[32,2048]{1,0:T(8,128)(2,1)S(1)} collective-permute-done((bf16[32,2048]{1,0:T(8,128)(2,1)}, bf16[32,2048]{1,0:T(8,128)(2,1)S(1)}, u32[]{:S(2)}, u32[]{:S(2)}) %collective-permute-start.23) | collective-permute-done | bytes 131104 | tf_op jit(solution)/shard_map/ppermute | solution.py:166
  94.5 3.4 %collective-permute-done.24.refs_10_ = bf16[32,2048]{1,0:T(8,128)(2,1)S(1)} collective-permute-done((bf16[32,2048]{1,0:T(8,128)(2,1)}, bf16[32,2048]{1,0:T(8,128)(2,1)S(1)}, u32[]{:S(2)}, u32[]{:S(2)}) %collective-permute-start.24) | collective-permute-done | bytes 131104 | tf_op jit(solution)/shard_map/ppermute | solution.py:166
  98.8 4.7 %shard_map.78 = (bf16[32,2048]{1,0:T(8,128)(2,1)}, bf16[32,2048]{1,0:T(8,128)(2,1)}, bf16[32,2048]{1,0:T(8,128)(2,1)}, bf16[32,2048]{1,0:T(8,128)(2,1)}, bf16[32...) custom-call(bf16[1,2048,512]{2,1,0:T(8,128)(2,1)} %refs_0_.3, ...), custom_call_target="tpu_custom_call" | custom-call | tf_op jit(solution)/shard_map/pallas_call | solution.py:171
  104.1 1.6 %collective-permute-start.27 = (bf16[32,2048]{1,0:T(8,128)(2,1)}, bf16[32,2048]{1,0:T(8,128)(2,1)S(1)}, u32[]{:S(2)}, u32[]{:S(2)}) collective-permute-start(bf16[32,2048]{1,0:T(8,128)(2,1)} %get-tuple-element.72), channel_id=1, source_target_pairs={{0,3},{1,2},{2,1},{3,0},{4,7},{5,6},{6,5},{7,4},{8,11},{9,10},{10,... | collective-permute-start | bytes 393224 | tf_op jit(solution)/shard_map/ppermute | solution.py:166
  108.8 3.4 %collective-permute-done.27.refs_3_ = bf16[32,2048]{1,0:T(8,128)(2,1)S(1)} collective-permute-done((bf16[32,2048]{1,0:T(8,128)(2,1)}, bf16[32,2048]{1,0:T(8,128)(2,1)S(1)}, u32[]{:S(2)}, u32[]{:S(2)}) %collective-permute-start.27) | collective-permute-done | bytes 131104 | tf_op jit(solution)/shard_map/ppermute | solution.py:166
  114.2 2.4 %collective-permute-done.30.refs_6_ = bf16[32,2048]{1,0:T(8,128)(2,1)S(1)} collective-permute-done((bf16[32,2048]{1,0:T(8,128)(2,1)}, bf16[32,2048]{1,0:T(8,128)(2,1)S(1)}, u32[]{:S(2)}, u32[]{:S(2)}) %collective-permute-start.30) | collective-permute-done | bytes 131104 | tf_op jit(solution)/shard_map/ppermute | solution.py:166
  116.6 3.1 %collective-permute-done.31.refs_7_ = bf16[32,2048]{1,0:T(8,128)(2,1)S(1)} collective-permute-done((bf16[32,2048]{1,0:T(8,128)(2,1)}, bf16[32,2048]{1,0:T(8,128)(2,1)S(1)}, u32[]{:S(2)}, u32[]{:S(2)}) %collective-permute-start.31) | collective-permute-done | bytes 131104 | tf_op jit(solution)/shard_map/ppermute | solution.py:166
  (66 shorter events, 29.7 us)
Async XLA Ops:
  0.0 28.2 %collective-permute-start.2 = (bf16[128,2048]{1,0:T(8,128)(2,1)}, bf16[128,2048]{1,0:T(8,128)(2,1)S(1)}, u32[]{:S(2)}, u32[]{:S(2)}) collective-permute-start(bf16[128,2048]{1,0:T(8,128)(2,1)} %hidden_ref.1), channel_id=1, source_target_pairs={{0,8},{8,0},{1,9},{9,1},{2,10},{10,2},{3,11},{11,3},{4,12},{12,4},... | collective-permute-start | bytes 1572872 | tf_op jit(solution)/shard_map/ppermute | solution.py:157
  2.3 23.1 %collective-permute-start = (s32[128,2]{0,1:T(2,128)}, s32[128,2]{0,1:T(2,128)S(1)}, u32[]{:S(2)}, u32[]{:S(2)}) collective-permute-start(s32[128,2]{0,1:T(2,128)} %param.8), channel_id=1, source_target_pairs={{0,8},{8,0},{1,9},{9,1},{2,10},{10,2},{3,11},{11,3},{4,12},{12,4},... | collective-permute-start | bytes 3080 | tf_op jit(solution)/shard_map/ppermute | solution.py:157
  30.6 8.3 %collective-permute-start.5 = (bf16[32,2048]{1,0:T(8,128)(2,1)}, bf16[32,2048]{1,0:T(8,128)(2,1)S(1)}, u32[]{:S(2)}, u32[]{:S(2)}) collective-permute-start(bf16[32,2048]{1,0:T(8,128)(2,1)} %get-tuple-element.48), channel_id=1, source_target_pairs={{0,3},{1,2},{2,1},{3,0},{4,7},{5,6},{6,5},{7,4},{8,11},{9,10},{10,... | collective-permute-start | bytes 393224 | tf_op jit(solution)/shard_map/ppermute | solution.py:166
  33.0 8.2 %collective-permute-start.7 = (bf16[32,2048]{1,0:T(8,128)(2,1)}, bf16[32,2048]{1,0:T(8,128)(2,1)S(1)}, u32[]{:S(2)}, u32[]{:S(2)}) collective-permute-start(bf16[32,2048]{1,0:T(8,128)(2,1)} %get-tuple-element.50), channel_id=1, source_target_pairs={{0,5},{1,4},{2,7},{3,6},{4,1},{5,0},{6,3},{7,2},{8,13},{9,12},{10,... | collective-permute-start | bytes 393224 | tf_op jit(solution)/shard_map/ppermute | solution.py:166
  33.8 8.8 %collective-permute-start.8 = (bf16[32,2048]{1,0:T(8,128)(2,1)}, bf16[32,2048]{1,0:T(8,128)(2,1)S(1)}, u32[]{:S(2)}, u32[]{:S(2)}) collective-permute-start(bf16[32,2048]{1,0:T(8,128)(2,1)} %get-tuple-element.51), channel_id=1, source_target_pairs={{0,6},{1,7},{2,4},{3,5},{4,2},{5,3},{6,0},{7,1},{8,14},{9,15},{10,... | collective-permute-start | bytes 393224 | tf_op jit(solution)/shard_map/ppermute | solution.py:166
  35.6 10.2 %collective-permute-start.9 = (bf16[32,2048]{1,0:T(8,128)(2,1)}, bf16[32,2048]{1,0:T(8,128)(2,1)S(1)}, u32[]{:S(2)}, u32[]{:S(2)}) collective-permute-start(bf16[32,2048]{1,0:T(8,128)(2,1)} %get-tuple-element.52), channel_id=1, source_target_pairs={{0,7},{1,6},{2,5},{3,4},{4,3},{5,2},{6,1},{7,0},{8,15},{9,14},{10,... | collective-permute-start | bytes 393224 | tf_op jit(solution)/shard_map/ppermute | solution.py:166
  51.4 8.2 %collective-permute-start.11 = (bf16[32,2048]{1,0:T(8,128)(2,1)}, bf16[32,2048]{1,0:T(8,128)(2,1)S(1)}, u32[]{:S(2)}, u32[]{:S(2)}) collective-permute-start(bf16[32,2048]{1,0:T(8,128)(2,1)} %get-tuple-element.55), channel_id=1, source_target_pairs={{0,2},{1,3},{2,0},{3,1},{4,6},{5,7},{6,4},{7,5},{8,10},{9,11},{10,... | collective-permute-start | bytes 393224 | tf_op jit(solution)/shard_map/ppermute | solution.py:166
  55.8 8.1 %collective-permute-start.12 = (bf16[32,2048]{1,0:T(8,128)(2,1)}, bf16[32,2048]{1,0:T(8,128)(2,1)S(1)}, u32[]{:S(2)}, u32[]{:S(2)}) collective-permute-start(bf16[32,2048]{1,0:T(8,128)(2,1)} %get-tuple-element.56), channel_id=1, source_target_pairs={{0,3},{1,2},{2,1},{3,0},{4,7},{5,6},{6,5},{7,4},{8,11},{9,10},{10,... | collective-permute-start | bytes 393224 | tf_op jit(solution)/shard_map/ppermute | solution.py:166
  56.9 8.6 %collective-permute-start.14 = (bf16[32,2048]{1,0:T(8,128)(2,1)}, bf16[32,2048]{1,0:T(8,128)(2,1)S(1)}, u32[]{:S(2)}, u32[]{:S(2)}) collective-permute-start(bf16[32,2048]{1,0:T(8,128)(2,1)} %get-tuple-element.58), channel_id=1, source_target_pairs={{0,5},{1,4},{2,7},{3,6},{4,1},{5,0},{6,3},{7,2},{8,13},{9,12},{10,... | collective-permute-start | bytes 393224 | tf_op jit(solution)/shard_map/ppermute | solution.py:166
  58.8 10.3 %collective-permute-start.15 = (bf16[32,2048]{1,0:T(8,128)(2,1)}, bf16[32,2048]{1,0:T(8,128)(2,1)S(1)}, u32[]{:S(2)}, u32[]{:S(2)}) collective-permute-start(bf16[32,2048]{1,0:T(8,128)(2,1)} %get-tuple-element.59), channel_id=1, source_target_pairs={{0,6},{1,7},{2,4},{3,5},{4,2},{5,3},{6,0},{7,1},{8,14},{9,15},{10,... | collective-permute-start | bytes 393224 | tf_op jit(solution)/shard_map/ppermute | solution.py:166
  59.6 12.3 %collective-permute-start.16 = (bf16[32,2048]{1,0:T(8,128)(2,1)}, bf16[32,2048]{1,0:T(8,128)(2,1)S(1)}, u32[]{:S(2)}, u32[]{:S(2)}) collective-permute-start(bf16[32,2048]{1,0:T(8,128)(2,1)} %get-tuple-element.60), channel_id=1, source_target_pairs={{0,7},{1,6},{2,5},{3,4},{4,3},{5,2},{6,1},{7,0},{8,15},{9,14},{10,... | collective-permute-start | bytes 393224 | tf_op jit(solution)/shard_map/ppermute | solution.py:166
  63.9 9.6 %collective-permute-start.18 = (bf16[32,2048]{1,0:T(8,128)(2,1)}, bf16[32,2048]{1,0:T(8,128)(2,1)S(1)}, u32[]{:S(2)}, u32[]{:S(2)}) collective-permute-start(bf16[32,2048]{1,0:T(8,128)(2,1)} %get-tuple-element.62), channel_id=1, source_target_pairs={{0,1},{1,0},{2,3},{3,2},{4,5},{5,4},{6,7},{7,6},{8,9},{9,8},{10,11... | collective-permute-start | bytes 393224 | tf_op jit(solution)/shard_map/ppermute | solution.py:166
  64.2 11.2 %collective-permute-start.19 = (bf16[32,2048]{1,0:T(8,128)(2,1)}, bf16[32,2048]{1,0:T(8,128)(2,1)S(1)}, u32[]{:S(2)}, u32[]{:S(2)}) collective-permute-start(bf16[32,2048]{1,0:T(8,128)(2,1)} %get-tuple-element.63), channel_id=1, source_target_pairs={{0,2},{1,3},{2,0},{3,1},{4,6},{5,7},{6,4},{7,5},{8,10},{9,11},{10,... | collective-permute-start | bytes 393224 | tf_op jit(solution)/shard_map/ppermute | solution.py:166
  65.5 12.0 %collective-permute-start.20 = (bf16[32,2048]{1,0:T(8,128)(2,1)}, bf16[32,2048]{1,0:T(8,128)(2,1)S(1)}, u32[]{:S(2)}, u32[]{:S(2)}) collective-permute-start(bf16[32,2048]{1,0:T(8,128)(2,1)} %get-tuple-element.64), channel_id=1, source_target_pairs={{0,3},{1,2},{2,1},{3,0},{4,7},{5,6},{6,5},{7,4},{8,11},{9,10},{10,... | collective-permute-start | bytes 393224 | tf_op jit(solution)/shard_map/ppermute | solution.py:166
  73.3 46.4 %collective-permute-start.17 = (bf16[128,2048]{1,0:T(8,128)(2,1)}, bf16[128,2048]{1,0:T(8,128)(2,1)S(1)}, u32[]{:S(2)}, u32[]{:S(2)}) collective-permute-start(bf16[128,2048]{1,0:T(8,128)(2,1)} %shard_map.76), channel_id=1, source_target_pairs={{0,8},{8,0},{1,9},{9,1},{2,10},{10,2},{3,11},{11,3},{4,12},{12,4},... | collective-permute-start | bytes 1572872 | tf_op jit(solution)/shard_map/ppermute | solution.py:157
  73.3 14.7 %collective-permute-start.21 = (bf16[32,2048]{1,0:T(8,128)(2,1)}, bf16[32,2048]{1,0:T(8,128)(2,1)S(1)}, u32[]{:S(2)}, u32[]{:S(2)}) collective-permute-start(bf16[32,2048]{1,0:T(8,128)(2,1)} %get-tuple-element.65), channel_id=1, source_target_pairs={{0,4},{1,5},{2,6},{3,7},{4,0},{5,1},{6,2},{7,3},{8,12},{9,13},{10,... | collective-permute-start | bytes 393224 | tf_op jit(solution)/shard_map/ppermute | solution.py:166
  73.4 19.0 %collective-permute-start.22 = (bf16[32,2048]{1,0:T(8,128)(2,1)}, bf16[32,2048]{1,0:T(8,128)(2,1)S(1)}, u32[]{:S(2)}, u32[]{:S(2)}) collective-permute-start(bf16[32,2048]{1,0:T(8,128)(2,1)} %get-tuple-element.66), channel_id=1, source_target_pairs={{0,5},{1,4},{2,7},{3,6},{4,1},{5,0},{6,3},{7,2},{8,13},{9,12},{10,... | collective-permute-start | bytes 393224 | tf_op jit(solution)/shard_map/ppermute | solution.py:166
  75.4 19.1 %collective-permute-start.23 = (bf16[32,2048]{1,0:T(8,128)(2,1)}, bf16[32,2048]{1,0:T(8,128)(2,1)S(1)}, u32[]{:S(2)}, u32[]{:S(2)}) collective-permute-start(bf16[32,2048]{1,0:T(8,128)(2,1)} %get-tuple-element.67), channel_id=1, source_target_pairs={{0,6},{1,7},{2,4},{3,5},{4,2},{5,3},{6,0},{7,1},{8,14},{9,15},{10,... | collective-permute-start | bytes 393224 | tf_op jit(solution)/shard_map/ppermute | solution.py:166
  77.5 20.4 %collective-permute-start.24 = (bf16[32,2048]{1,0:T(8,128)(2,1)}, bf16[32,2048]{1,0:T(8,128)(2,1)S(1)}, u32[]{:S(2)}, u32[]{:S(2)}) collective-permute-start(bf16[32,2048]{1,0:T(8,128)(2,1)} %get-tuple-element.68), channel_id=1, source_target_pairs={{0,7},{1,6},{2,5},{3,4},{4,3},{5,2},{6,1},{7,0},{8,15},{9,14},{10,... | collective-permute-start | bytes 393224 | tf_op jit(solution)/shard_map/ppermute | solution.py:166
  104.1 8.1 %collective-permute-start.27 = (bf16[32,2048]{1,0:T(8,128)(2,1)}, bf16[32,2048]{1,0:T(8,128)(2,1)S(1)}, u32[]{:S(2)}, u32[]{:S(2)}) collective-permute-start(bf16[32,2048]{1,0:T(8,128)(2,1)} %get-tuple-element.72), channel_id=1, source_target_pairs={{0,3},{1,2},{2,1},{3,0},{4,7},{5,6},{6,5},{7,4},{8,11},{9,10},{10,... | collective-permute-start | bytes 393224 | tf_op jit(solution)/shard_map/ppermute | solution.py:166
  105.7 7.5 %collective-permute-start.28 = (bf16[32,2048]{1,0:T(8,128)(2,1)}, bf16[32,2048]{1,0:T(8,128)(2,1)S(1)}, u32[]{:S(2)}, u32[]{:S(2)}) collective-permute-start(bf16[32,2048]{1,0:T(8,128)(2,1)} %get-tuple-element.73), channel_id=1, source_target_pairs={{0,4},{1,5},{2,6},{3,7},{4,0},{5,1},{6,2},{7,3},{8,12},{9,13},{10,... | collective-permute-start | bytes 393224 | tf_op jit(solution)/shard_map/ppermute | solution.py:166
  105.7 8.5 %collective-permute-start.29 = (bf16[32,2048]{1,0:T(8,128)(2,1)}, bf16[32,2048]{1,0:T(8,128)(2,1)S(1)}, u32[]{:S(2)}, u32[]{:S(2)}) collective-permute-start(bf16[32,2048]{1,0:T(8,128)(2,1)} %get-tuple-element.74), channel_id=1, source_target_pairs={{0,5},{1,4},{2,7},{3,6},{4,1},{5,0},{6,3},{7,2},{8,13},{9,12},{10,... | collective-permute-start | bytes 393224 | tf_op jit(solution)/shard_map/ppermute | solution.py:166
  108.5 8.1 %collective-permute-start.30 = (bf16[32,2048]{1,0:T(8,128)(2,1)}, bf16[32,2048]{1,0:T(8,128)(2,1)S(1)}, u32[]{:S(2)}, u32[]{:S(2)}) collective-permute-start(bf16[32,2048]{1,0:T(8,128)(2,1)} %get-tuple-element.75), channel_id=1, source_target_pairs={{0,6},{1,7},{2,4},{3,5},{4,2},{5,3},{6,0},{7,1},{8,14},{9,15},{10,... | collective-permute-start | bytes 393224 | tf_op jit(solution)/shard_map/ppermute | solution.py:166
  112.2 7.5 %collective-permute-start.31 = (bf16[32,2048]{1,0:T(8,128)(2,1)}, bf16[32,2048]{1,0:T(8,128)(2,1)S(1)}, u32[]{:S(2)}, u32[]{:S(2)}) collective-permute-start(bf16[32,2048]{1,0:T(8,128)(2,1)} %get-tuple-element.76), channel_id=1, source_target_pairs={{0,7},{1,6},{2,5},{3,4},{4,3},{5,2},{6,1},{7,0},{8,15},{9,14},{10,... | collective-permute-start | bytes 393224 | tf_op jit(solution)/shard_map/ppermute | solution.py:166
  (17 other events, 147.5 us)
